TPU v7x, 32 devices: a whole 2x2x4 slice. The times are simulated.
32 devices in a mesh: sp: 4 (over y, x), tp: 8 (over z, core).
Axes of the slice: x: 2, y: 2, z: 4, core: 2. Of those that a mesh axis runs over, the one named last changes fastest.
Arguments:
- layer_input: bfloat16 [2048, 2048], P(('sp', 'tp')), may hold values from -6 to 6
- receptance: bfloat16 [2048, 2048], P('sp', 'tp'), may hold values from -6 to 6
- keys: bfloat16 [2048, 2048], P('sp', 'tp'), may hold values from -6 to 6
- values: bfloat16 [2048, 2048], P('sp', 'tp'), may hold values from -6 to 6
- erase_preact: bfloat16 [2048, 2048], P('sp', 'tp'), may hold values from -12 to 5
- decay_preact: bfloat16 [2048, 2048], P('sp', 'tp'), may hold values from -40 to 3
- decay_spike: float32 [2048, 32], P('sp', 'tp'), may hold values from -2 to 0
- head_norm_gain: bfloat16 [2048], P('tp'), may hold values from 0.099609375 to 1.8984375
- output_weight: bfloat16 [2048, 2048], P('tp'), may hold values from -0.125 to 0.125
- expert_norm_gain: bfloat16 [2048], replicated, may hold values from 0.099609375 to 1.8984375
- routes: int32 [2048, 2], P(('sp', 'tp')), may hold values from 0 to 7, all different within a row; in each aligned block of 64 rows (0 to 63, 64 to 127, ...) at most 24 rows name the same one
- routing_weight: float32 [2048, 2], P(('sp', 'tp')), may hold values from 0.3 to 1.5
- expert_gate_weight: bfloat16 [8, 2048, 4096], P('sp', None, 'tp'), may hold values from -0.125 to 0.125
- expert_up_weight: bfloat16 [8, 2048, 4096], P('sp', None, 'tp'), may hold values from -0.125 to 0.125
- expert_down_weight: bfloat16 [8, 4096, 2048], P('sp', 'tp'), may hold values from -0.09375 to 0.09375
- shared_gate_weight: bfloat16 [2048, 4096], P(None, 'tp'), may hold values from -0.125 to 0.125
- shared_up_weight: bfloat16 [2048, 4096], P(None, 'tp'), may hold values from -0.125 to 0.125
- shared_down_weight: bfloat16 [4096, 2048], P('tp'), may hold values from -0.09375 to 0.09375
Outputs:
- layer_out: bfloat16 [2048, 2048], P(('sp', 'tp'))
Inputs may be any that keep to these rules, and one draw needn't show every extreme that they name: `routes`: in each aligned block of 64 rows no expert is named by more than 24 rows.
All inputs are finite; a program needn't handle non-finite values.
Results may differ from a plain program's by a relative error of at most 0.02.
Values may be sent and summed in bfloat16 or wider, within the bound.
A program may use at most 128 MiB of HBM per device.

v0:
```python
import jax
import jax.numpy as jnp
from jax import lax
from jax.sharding import PartitionSpec as P

BLOCK = 64


highest = lax.Precision.HIGHEST
GN_EPS = 0.00064
RMS_EPS = 1e-06


def product(left, right):
    return jnp.einsum("...ij,...jk->...ik", left, right, precision=highest)


def unit_inverse(strict, row_ids, col_ids, identity):
    length = strict.shape[-1]
    size, inverse = 1, identity
    while size < length:
        joined = row_ids // (2 * size) == col_ids // (2 * size)
        corner = jnp.where(joined & (row_ids // size != col_ids // size), strict, 0.0)
        if size == 1:
            inverse = identity - corner
        else:
            inverse = inverse - product(inverse, product(corner, inverse))
        size *= 2
    return inverse


def flip_second(array):
    return jnp.stack([array[0], array[1, ::-1]])


def mixer(decay_logarithm, unit_keys, beta, key_rows, value_rows, read_rows):
    tokens_here, head_number, width = key_rows.shape
    span = BLOCK
    block_count = tokens_here // span

    def to_blocks(array):
        return jnp.swapaxes(array.reshape(block_count, span, head_number, width), 1, 2)

    decay_logarithm, unit_keys, beta, key_rows, value_rows, read_rows = [
        to_blocks(array)
        for array in (decay_logarithm, unit_keys, beta, key_rows, value_rows, read_rows)
    ]
    row_ids = lax.broadcasted_iota(jnp.int32, (span, span), 0)
    col_ids = lax.broadcasted_iota(jnp.int32, (span, span), 1)
    identity = (row_ids == col_ids).astype(jnp.float32)
    strict = jnp.stack([row_ids > col_ids, row_ids < col_ids])
    loose = strict | (row_ids == col_ids)
    cumulative = jnp.einsum(
        "dts,bhsn->dbhtn", loose.astype(jnp.float32), decay_logarithm, precision=highest
    )
    total = jnp.sum(decay_logarithm, axis=2, keepdims=True)
    middle = 0.5 * total
    left_scale = jnp.exp(cumulative - middle)
    before_scale = jnp.exp(cumulative - decay_logarithm - middle)
    right_scale = jnp.exp(middle - cumulative)
    end_scale = jnp.exp(total - cumulative)
    middle_scale = jnp.exp(middle)
    left = jnp.concatenate([unit_keys * before_scale, read_rows * left_scale], axis=-2)
    right = jnp.concatenate([beta * right_scale, key_rows * right_scale], axis=-2)
    keep = jnp.concatenate([strict, loose], axis=-2)
    keep = jnp.concatenate([keep, keep], axis=-1)[:, None, None]
    scores = jnp.einsum("...tn,...sn->...ts", left, right, precision=highest)
    scores = jnp.where(keep, scores, 0.0)
    true_left = left * middle_scale
    both_values = jnp.broadcast_to(value_rows, (2,) + value_rows.shape)
    key_part = product(scores[..., span:], both_values)
    inverse = unit_inverse(scores[..., :span, :span], row_ids, col_ids, identity)
    right_side = jnp.concatenate([true_left[..., :span, :], -key_part[..., :span, :]], axis=-1)
    solved = product(inverse, right_side)
    read_solved = product(scores[..., span:, :span], solved)
    local = read_solved[..., width:] + key_part[..., span:, :]
    readout = true_left[..., span:, :] - read_solved[..., :width]
    solved_end = jnp.einsum("...tv,...tm->...vm", solved, beta * end_scale, precision=highest)
    value_end = jnp.einsum(
        "...tv,...tm->...vm", both_values, key_rows * end_scale, precision=highest
    )
    eye = jnp.eye(width, dtype=jnp.float32)
    diagonal = jnp.exp(total)[:, :, 0, :, None] * eye
    maps = jnp.concatenate(
        [diagonal - solved_end[..., :width, :], solved_end[..., width:, :] + value_end], axis=-2
    )
    maps = flip_second(maps)
    shift = 1
    while shift < block_count:
        later = maps[:, shift:]
        carry = jnp.concatenate(
            [jnp.zeros_like(later[..., :width, :]), later[..., width:, :]], axis=-2
        )
        moved = product(maps[:, :-shift], later[..., :width, :]) + carry
        maps = jnp.concatenate([maps[:, :shift], moved], axis=1)
        shift *= 2
    size, place = lax.axis_size("sp"), lax.axis_index("sp")
    everything = lax.all_gather(maps[:, -1].astype(jnp.bfloat16), "sp").astype(jnp.float32)
    entry = jnp.zeros((2, head_number, width, width), jnp.float32)
    which = lax.broadcasted_iota(jnp.int32, (2, 1, 1, 1), 0)
    for k in range(size):
        part = jnp.stack([everything[k, 0], everything[size - 1 - k, 1]])
        moved = product(entry, part[..., :width, :]) + part[..., width:, :]
        reached = jnp.where(which == 0, k < place, size - 1 - k > place)
        entry = jnp.where(reached, moved, entry)
    first = jnp.concatenate([eye, jnp.zeros_like(eye)], axis=0)
    first = jnp.broadcast_to(first, maps[:, :1].shape)
    prefix = jnp.concatenate([first, maps[:, :-1]], axis=1)
    whole_entry = jnp.broadcast_to(entry[:, None], prefix[..., :width, :].shape)
    starts = product(whole_entry, prefix[..., :width, :]) + prefix[..., width:, :]
    starts = flip_second(starts)
    result = local + jnp.einsum("...tn,...vn->...tv", readout, starts, precision=highest)
    mix = result[0] + result[1]
    center = jnp.mean(mix, axis=-1, keepdims=True)
    spread = jnp.mean(jnp.square(mix - center), axis=-1, keepdims=True)
    mixed = (mix - center) * lax.rsqrt(spread + GN_EPS)
    return jnp.swapaxes(mixed, 1, 2).reshape(tokens_here, head_number * width)


def body(
    layer_input,
    receptance,
    keys,
    values,
    erase_preact,
    decay_preact,
    decay_spike,
    head_norm_gain,
    output_weight,
    expert_norm_gain,
    routes,
    routing_weight,
    expert_gate_weight,
    expert_up_weight,
    expert_down_weight,
    shared_gate_weight,
    shared_up_weight,
    shared_down_weight,
):
    tokens_here = keys.shape[0]
    head_number = decay_spike.shape[1]
    head_width = keys.shape[1] // head_number

    def each_head(array):
        return array.astype(jnp.float32).reshape(tokens_here, head_number, head_width)

    key_rows = each_head(keys)
    unit_keys = key_rows * lax.rsqrt(jnp.sum(key_rows * key_rows, axis=-1, keepdims=True) + 1e-06)
    beta = unit_keys * jax.nn.sigmoid(each_head(erase_preact))
    decay_logarithm = (
        -jnp.exp(-jax.nn.softplus(-each_head(decay_preact)) - 0.5) + decay_spike[:, :, None]
    )
    arrays = (decay_logarithm, unit_keys, beta, key_rows, each_head(values), each_head(receptance))
    mixed = mixer(*arrays)
    mixed = (mixed * head_norm_gain.astype(jnp.float32)).astype(jnp.bfloat16)
    row_count = layer_input.shape[0]
    model_width = layer_input.shape[1]
    slab = mixed
    projected = lax.psum_scatter(
        jnp.dot(slab, output_weight, preferred_element_type=jnp.float32).astype(jnp.bfloat16),
        "tp",
        scatter_dimension=0,
        tiled=True,
    ).astype(jnp.float32)
    residual = layer_input.astype(jnp.float32) + projected
    normed = residual * lax.rsqrt(jnp.mean(residual * residual, axis=-1, keepdims=True) + RMS_EPS)
    normed = (normed * expert_norm_gain.astype(jnp.float32)).astype(jnp.bfloat16)
    everyone = lax.all_gather(normed, "tp", axis=0, tiled=True)
    top_count = routes.shape[1]
    expert_local = expert_gate_weight.shape[0]
    sp_count = lax.axis_size("sp")
    expert_total = expert_local * sp_count
    capacity = max(2, (3 * row_count * top_count + 2 * expert_total - 1) // (2 * expert_total))
    slot_total = sp_count * capacity * expert_local
    entries = routes.reshape(-1)
    entry_count = entries.shape[0]
    expert_hot = (entries[:, None] == lax.broadcasted_iota(jnp.int32, (1, expert_total), 1)).astype(
        jnp.int32
    )
    rank_in = jnp.sum((jnp.cumsum(expert_hot, axis=0) - 1) * expert_hot, axis=1)
    slot_of = entries * capacity + rank_in
    slot_hot = (slot_of[:, None] == lax.broadcasted_iota(jnp.int32, (1, slot_total), 1)).astype(
        jnp.float32
    )
    owner_hot = (
        lax.broadcasted_iota(jnp.int32, (entry_count, 1), 0) // top_count
        == lax.broadcasted_iota(jnp.int32, (1, row_count), 1)
    ).astype(jnp.float32)
    placing = jnp.dot(slot_hot.T, owner_hot, precision=highest)
    weighting = jnp.dot(owner_hot.T, slot_hot * routing_weight.reshape(-1, 1), precision=highest)
    outgoing = jnp.dot(placing.astype(jnp.bfloat16), normed, preferred_element_type=jnp.float32)
    outgoing = outgoing.astype(jnp.bfloat16).reshape(sp_count, expert_local, capacity, model_width)
    arrived = lax.all_to_all(outgoing, "sp", split_axis=0, concat_axis=0, tiled=True)

    def gathered(rows):
        return lax.all_gather(rows, "tp", axis=0, tiled=True)

    def hidden_layer(rows, gate, up, down):
        gate_value = jnp.dot(rows, gate, preferred_element_type=jnp.float32)
        up_value = jnp.dot(rows, up, preferred_element_type=jnp.float32)
        hidden = (jax.nn.silu(gate_value) * up_value).astype(jnp.bfloat16)
        partial_rows = jnp.dot(hidden, down, preferred_element_type=jnp.float32)
        return lax.psum_scatter(
            partial_rows.astype(jnp.bfloat16), "tp", scatter_dimension=0, tiled=True
        )

    shared = hidden_layer(everyone, shared_gate_weight, shared_up_weight, shared_down_weight)
    routed_rows = []
    for j in range(expert_local):
        rows = gathered(arrived[:, j].reshape(sp_count * capacity, model_width))
        out = hidden_layer(
            rows, expert_gate_weight[j], expert_up_weight[j], expert_down_weight[j]
        )
        routed_rows.append(out.reshape(sp_count, 1, capacity, model_width))
    routed_rows = jnp.concatenate(routed_rows, axis=1)
    returned = lax.all_to_all(routed_rows, "sp", split_axis=0, concat_axis=0, tiled=True)
    routed = jnp.dot(
        weighting, returned.reshape(slot_total, model_width).astype(jnp.float32), precision=highest
    )
    return (residual + shared.astype(jnp.float32) + routed).astype(jnp.bfloat16)


def solution(mesh):
    return jax.shard_map(
        body,
        mesh=mesh,
        in_specs=(
            P(("sp", "tp"), None),
            P("sp", "tp"),
            P("sp", "tp"),
            P("sp", "tp"),
            P("sp", "tp"),
            P("sp", "tp"),
            P("sp", "tp"),
            P("tp"),
            P("tp", None),
            P(),
            P(("sp", "tp"), None),
            P(("sp", "tp"), None),
            P("sp", None, "tp"),
            P("sp", None, "tp"),
            P("sp", "tp", None),
            P(None, "tp"),
            P(None, "tp"),
            P("tp", None),
        ),
        out_specs=P(("sp", "tp"), None),
        check_vma=False,
    )
```

profile of v0, /device:TPU:0, one launch (start us, length us, event | category | flops | bytes accessed | tf_op | source)
XLA Modules:
  0.0 474.2 jit_solution(114120175428504890)
XLA Ops:
  33.9 4.4 fusion.70
  40.8 7.3 %convolution_select_fusion = f32[2,8,4,128,128]{3,4,2,1,0:T(8,128)S(1)} fusion(f32[2,8,4,128,64]{3,4,0,2,1:T(8,128)S(1)} %get-tuple-element.6, pred[2,128,128]{1,2,0:T(8,128)(4,1)S(1)} %copy.117, f32[2,8,4,64,64]{3,4,0,2,1:T(8,128)S(1)} %get-tuple-element.15, f32[2,8,4,64,64]{3,4,0,2,1:T(8,128)S(1)} %get-tuple-element.14), kind=kOutput, calls=%fused_computation.18 | convolution fusion | flops 806879232 | bytes 8421376 | tf_op jit(solution)/shard_map/...tn,...sn->...ts/dot_general | solution.py:67
  81.3 4.9 %fusion.202 = f32[2,8,4,64,64]{3,4,2,1,0:T(8,128)} fusion(f32[2,8,4,64,64]{3,4,2,1,0:T(8,128)S(1)} %convolution_subtract_fusion, f32[2,8,4,64,64]{4,3,2,1,0:T(8,128)S(1)} %fusion.57), kind=kOutput, calls=%fused_computation.323 | convolution fusion | flops 201326592 | bytes 3145728 | tf_op jit(solution)/shard_map/...ij,...jk->...ik/dot_general | solution.py:15
  86.8 5.6 %fusion.12 = f32[2,8,4,128,64]{3,4,2,1,0:T(8,128)S(1)} fusion(f32[2,8,4,128,128]{3,4,2,1,0:T(8,128)} %copy-done.1, f32[8,4,64,64]{3,2,1,0:T(8,128)S(1)} %copy.152), kind=kOutput, calls=%fused_computation.34 | convolution fusion | flops 402653184 | bytes 4718592 | tf_op jit(solution)/shard_map/...ij,...jk->...ik/dot_general | solution.py:15
  95.4 8.2 %fusion = f32[2,8,4,64,128]{4,3,2,1,0:T(8,128)S(1)} fusion(f32[2,8,4,64,64]{3,4,2,1,0:T(8,128)S(1)} %copy-done.4, f32[2,8,4,64,64]{3,4,2,1,0:T(8,128)S(1)} %copy-done.14, f32[2,8,4,64,64]{3,4,0,2,1:T(8,128)S(1)} %copy_negate_fusion, f32[2,8,4,64,64]{3,4,0,2,1:T(8,128)S(1)} %bitcast.162), kind=kOutput, calls=%fused_computation.1 | convolution fusion | flops 403439616 | bytes 6291456 | tf_op jit(solution)/shard_map/...ij,...jk->...ik/dot_general | solution.py:15
  121.8 4.0 pad_add_fusion.1
  130.4 5.6 %fusion.14 = f32[2,8,4,64,128]{4,3,2,1,0:T(8,128)} fusion(f32[2,8,4,64,128]{4,3,2,1,0:T(8,128)S(1)} %copy-done.6, f32[2,8,4,128,128]{3,4,2,1,0:T(8,128)S(1)} %copy-done.2), kind=kOutput, calls=%fused_computation.36 | convolution fusion | flops 402653184 | bytes 6291456 | tf_op jit(solution)/shard_map/...ij,...jk->...ik/dot_general | solution.py:15
  135.9 11.7 %all-gather = bf16[8,1,4,128,64]{3,4,2,1,0:T(8,128)(2,1)S(1)} all-gather(bf16[2,1,4,128,64]{3,4,2,1,0:T(8,128)(2,1)S(1)} %slice.447), channel_id=2, replica_groups=mesh['sp'=4,'tp'=8] {'sp'}, dimensions={0}, use_global_device_ids=true | all-gather | bytes 655360 | tf_op jit(solution)/shard_map/all_gather | solution.py:98
  159.5 5.1 %fusion.198 = (f32[2,8,4,64,64]{4,3,2,1,0:T(8,128)}, f32[2,8,4,64,64]{4,3,2,1,0:T(8,128)}) fusion(f32[2,8,4,64,128]{4,3,2,1,0:T(8,128)} %fusion.14), kind=kLoop, calls=%fused_computation.319 | loop fusion | bytes 4194304 | tf_op jit(solution)/shard_map/slice | solution.py:77
  170.5 8.2 %fusion.11 = f32[2,8,4,64,64]{3,4,2,1,0:T(8,128)S(1)} fusion(f32[2,8,4,64,64]{3,4,2,1,0:T(8,128)} %copy.205, f32[2,8,4,128,64]{3,4,2,1,0:T(8,128)} %copy-done.8, f32[1,8,4,64,64]{3,4,2,1,0:T(8,128)S(1)} %rev.7, f32[1,8,4,64,64]{3,4,2,1,0:T(8,128)} %get-tuple-element.21, f32[2,8,4,64,64]{3,4,0,2,1:T(8,128)} %copy.206, f32[2,8,4,128,64]{3,4,0,2,1:T(8,128)} %get-tuple-element.5), kind=kOutput, calls=%fused_computation.33 | convolution fusion | flops 202375168 | bytes 7340032 | tf_op jit(solution)/shard_map/...tn,...vn->...tv/dot_general | solution.py:112
  186.1 35.5 %reduce-scatter.5.cloned.1.call-done = bf16[64,2048]{1,0:T(8,128)(2,1)} async-done(((bf16[512,2048]{1,0:T(8,128)(2,1)}), bf16[64,2048]{1,0:T(8,128)(2,1)}) %reduce-scatter.5.cloned.1.call-update) | async-done | bytes 262160 | tf_op jit(solution)/shard_map/reduce_scatter | solution.py:159
  224.2 12.0 %all_to_all.10 = bf16[4,2,24,2048]{3,2,1,0:T(8,128)(2,1)S(1)} all-to-all(bf16[4,2,24,2048]{3,2,1,0:T(8,128)(2,1)S(1)} %bitcast.166), channel_id=1, replica_groups=mesh['sp'=4,'tp'=8] {'sp'}, dimensions={0} | all-to-all | bytes 1572864 | tf_op jit(solution)/shard_map/all_to_all | solution.py:193
  238.8 36.1 %all-gather.7.cloned.1.call-done = bf16[768,2048]{1,0:T(8,128)(2,1)} async-done(((bf16[96,2048]{1,0:T(8,128)(2,1)}), bf16[768,2048]{1,0:T(8,128)(2,1)}) %all-gather.7.cloned.1.call-update) | async-done | bytes 3145744 | tf_op jit(solution)/shard_map/all_gather | solution.py:196
  274.9 5.5 %fusion.34 = f32[768,512]{1,0:T(8,128)} fusion(bf16[768,2048]{1,0:T(8,128)(2,1)} %all-gather.7.cloned.1.call-done, bf16[2,2048,512]{2,1,0:T(8,128)(2,1)} %param.30), kind=kOutput, calls=%fused_computation.61 | convolution fusion | flops 1610612736 | bytes 6815744 | tf_op jit(solution)/shard_map/dot_general | solution.py:199
  280.4 9.3 %convolution_convert_fusion.1 = bf16[768,2048]{1,0:T(8,128)(2,1)} fusion(bf16[2,512,2048]{2,1,0:T(8,128)(2,1)} %param.32, f32[768,512]{1,0:T(8,128)} %fusion.34, bf16[768,2048]{1,0:T(8,128)(2,1)} %all-gather.7.cloned.1.call-done, bf16[2,2048,512]{2,1,0:T(8,128)(2,1)} %param.31), kind=kOutput, calls=%fused_computation.4 | convolution fusion | flops 3225157632 | bytes 12058624 | tf_op jit(solution)/shard_map/dot_general | solution.py:202
  289.7 23.9 %all-gather.9.cloned.1.call-done = bf16[768,2048]{1,0:T(8,128)(2,1)} async-done(((bf16[96,2048]{1,0:T(8,128)(2,1)}), bf16[768,2048]{1,0:T(8,128)(2,1)}) %all-gather.9.cloned.1.call-update) | async-done | bytes 3145744 | tf_op jit(solution)/shard_map/all_gather | solution.py:196
  313.6 5.5 %fusion.29 = f32[768,512]{1,0:T(8,128)} fusion(bf16[768,2048]{1,0:T(8,128)(2,1)} %all-gather.9.cloned.1.call-done, bf16[2,2048,512]{2,1,0:T(8,128)(2,1)} %param.30), kind=kOutput, calls=%fused_computation.56 | convolution fusion | flops 1610612736 | bytes 6815744 | tf_op jit(solution)/shard_map/dot_general | solution.py:199
  319.2 9.2 %convolution_convert_fusion = bf16[768,2048]{1,0:T(8,128)(2,1)} fusion(bf16[2,512,2048]{2,1,0:T(8,128)(2,1)} %param.32, f32[768,512]{1,0:T(8,128)} %fusion.29, bf16[768,2048]{1,0:T(8,128)(2,1)} %all-gather.9.cloned.1.call-done, bf16[2,2048,512]{2,1,0:T(8,128)(2,1)} %param.31), kind=kOutput, calls=%fused_computation.3 | convolution fusion | flops 3225157632 | bytes 12058624 | tf_op jit(solution)/shard_map/dot_general | solution.py:202
  328.5 14.7 %all-gather.5.cloned.1.call-done = bf16[512,2048]{1,0:T(8,128)(2,1)} async-done(((bf16[64,2048]{1,0:T(8,128)(2,1)}), bf16[512,2048]{1,0:T(8,128)(2,1)}) %all-gather.5.cloned.1.call-update) | async-done | bytes 2097168 | tf_op jit(solution)/shard_map/all_gather | solution.py:168
  343.2 4.5 fusion.203
  347.7 6.3 %convolution_convert_fusion.3 = bf16[512,2048]{1,0:T(8,128)(2,1)} fusion(bf16[512,2048]{1,0:T(8,128)(2,1)S(1)} %copy-done, bf16[512,2048]{1,0:T(8,128)(2,1)} %all-gather.5.cloned.1.call-done, bf16[2048,512]{1,0:T(8,128)(2,1)} %param.34, f32[512,512]{1,0:T(8,128)} %fusion.203), kind=kOutput, calls=%fused_computation.14 | convolution fusion | flops 2150105088 | bytes 9437184 | tf_op jit(solution)/shard_map/dot_general | solution.py:202
  354.0 31.2 %reduce-scatter.9.cloned.1.call-done = bf16[96,2048]{1,0:T(8,128)(2,1)} async-done(((bf16[768,2048]{1,0:T(8,128)(2,1)}), bf16[96,2048]{1,0:T(8,128)(2,1)}) %reduce-scatter.9.cloned.1.call-update) | async-done | bytes 393232 | tf_op jit(solution)/shard_map/reduce_scatter | solution.py:203
  385.1 41.9 %reduce-scatter.11.cloned.1.call-done = bf16[96,2048]{1,0:T(8,128)(2,1)} async-done(((bf16[768,2048]{1,0:T(8,128)(2,1)}), bf16[96,2048]{1,0:T(8,128)(2,1)}) %reduce-scatter.11.cloned.1.call-update) | async-done | bytes 393232 | tf_op jit(solution)/shard_map/reduce_scatter | solution.py:203
  433.3 31.6 %reduce-scatter.7.cloned.1.call-done = bf16[64,2048]{1,0:T(8,128)(2,1)} async-done(((bf16[512,2048]{1,0:T(8,128)(2,1)}), bf16[64,2048]{1,0:T(8,128)(2,1)}) %reduce-scatter.7.cloned.1.call-update) | async-done | bytes 262160 | tf_op jit(solution)/shard_map/reduce_scatter | solution.py:203
  (220 shorter events, 127.3 us)
Async XLA Ops:
  6.5 341.1 %copy-start = (bf16[512,2048]{1,0:T(8,128)(2,1)S(1)}, bf16[512,2048]{1,0:T(8,128)(2,1)}, u32[]{:S(2)}) copy-start(bf16[512,2048]{1,0:T(8,128)(2,1)} %param.35) | copy-start | bytes 6291460
  6.5 7.8 %copy-start.20 = (bf16[512,256]{1,0:T(8,128)(2,1)S(1)}, bf16[512,256]{1,0:T(8,128)(2,1)}, u32[]{:S(2)}) copy-start(bf16[512,256]{1,0:T(8,128)(2,1)} %param.23) | copy-start | bytes 786436
  6.5 215.0 %reduce-scatter.5.cloned.1.call-start = ((), (), s32[]{:S(2)}) async-start(), calls=%async_computation.6 | async-start | bytes 2359296 | tf_op jit(solution)/shard_map/reduce_scatter | solution.py:159
  40.7 7.5 %copy-start.31 = (pred[64]{0:T(512)(128)(4,1)S(1)}, pred[64]{0:T(512)(128)(4,1)}, u32[]{:S(2)}) copy-start(pred[64]{0:T(512)(128)(4,1)} %get-tuple-element.51) | copy-start | bytes 196
  40.7 7.5 %copy-start.32 = (pred[64]{0:T(512)(128)(4,1)S(1)}, pred[64]{0:T(512)(128)(4,1)}, u32[]{:S(2)}) copy-start(pred[64]{0:T(512)(128)(4,1)} %get-tuple-element.52) | copy-start | bytes 196
  40.7 7.5 %copy-start.33 = (s32[64]{0:T(128)S(1)}, s32[64]{0:T(128)}, u32[]{:S(2)}) copy-start(s32[64]{0:T(128)} %get-tuple-element.53) | copy-start | bytes 772
  40.7 7.5 %copy-start.34 = (s32[64]{0:T(128)S(1)}, s32[64]{0:T(128)}, u32[]{:S(2)}) copy-start(s32[64]{0:T(128)} %get-tuple-element.54) | copy-start | bytes 772
  40.7 7.5 %copy-start.35 = (s32[64]{0:T(128)S(1)}, s32[64]{0:T(128)}, u32[]{:S(2)}) copy-start(s32[64]{0:T(128)} %get-tuple-element.55) | copy-start | bytes 772
  40.7 7.5 %copy-start.36 = (s32[64]{0:T(128)S(1)}, s32[64]{0:T(128)}, u32[]{:S(2)}) copy-start(s32[64]{0:T(128)} %get-tuple-element.56) | copy-start | bytes 772
  40.7 7.5 %copy-start.37 = (s32[64]{0:T(128)S(1)}, s32[64]{0:T(128)}, u32[]{:S(2)}) copy-start(s32[64]{0:T(128)} %get-tuple-element.57) | copy-start | bytes 772
  40.7 7.5 %copy-start.38 = (s32[64]{0:T(128)S(1)}, s32[64]{0:T(128)}, u32[]{:S(2)}) copy-start(s32[64]{0:T(128)} %get-tuple-element.58) | copy-start | bytes 772
  48.1 29.5 %copy-start.1 = (f32[2,8,4,128,128]{3,4,2,1,0:T(8,128)}, f32[2,8,4,128,128]{3,4,2,1,0:T(8,128)S(1)}, u32[]{:S(2)}) copy-start(f32[2,8,4,128,128]{3,4,2,1,0:T(8,128)S(1)} %convolution_select_fusion) | copy-start | bytes 12582916
  95.4 8.2 %copy-start.13 = (f32[2,8,4,64,64]{3,4,0,2,1:T(8,128)S(1)}, f32[2,8,4,64,64]{3,4,0,2,1:T(8,128)}, u32[]{:S(2)}) copy-start(f32[2,8,4,64,64]{3,4,0,2,1:T(8,128)} %get-tuple-element.13) | copy-start | bytes 3145732
  185.0 36.5 %copy-start.18 = (bf16[64,2048]{1,0:T(8,128)(2,1)S(1)}, bf16[64,2048]{1,0:T(8,128)(2,1)}, u32[]{:S(2)}) copy-start(bf16[64,2048]{1,0:T(8,128)(2,1)} %param.18) | copy-start | bytes 786436
  185.0 89.8 %all-gather.7.cloned.1.call-start = ((), (), s32[]{:S(2)}) async-start(), calls=%async_computation.9 | async-start | bytes 3538944 | tf_op jit(solution)/shard_map/all_gather | solution.py:196
  223.8 13.4 %copy-start.17 = (bf16[64,2048]{1,0:T(8,128)(2,1)}, bf16[64,2048]{1,0:T(8,128)(2,1)S(1)}, u32[]{:S(2)}) copy-start(bf16[64,2048]{1,0:T(8,128)(2,1)S(1)} %multiply_convert_fusion.2) | copy-start | bytes 786436
  237.2 76.4 %all-gather.9.cloned.1.call-start = ((), (), s32[]{:S(2)}) async-start(), calls=%async_computation.11 | async-start | bytes 3538944 | tf_op jit(solution)/shard_map/all_gather | solution.py:196
  237.9 105.3 %all-gather.5.cloned.1.call-start = ((), (), s32[]{:S(2)}) async-start(), calls=%async_computation.7 | async-start | bytes 2359296 | tf_op jit(solution)/shard_map/all_gather | solution.py:168
  238.5 146.6 %reduce-scatter.9.cloned.1.call-start = ((), (), s32[]{:S(2)}) async-start(), calls=%async_computation.10 | async-start | bytes 3538944 | tf_op jit(solution)/shard_map/reduce_scatter | solution.py:203
  289.7 137.4 %reduce-scatter.11.cloned.1.call-start = ((), (), s32[]{:S(2)}) async-start(), calls=%async_computation.12 | async-start | bytes 3538944 | tf_op jit(solution)/shard_map/reduce_scatter | solution.py:203
  328.4 136.5 %reduce-scatter.7.cloned.1.call-start = ((), (), s32[]{:S(2)}) async-start(), calls=%async_computation.8 | async-start | bytes 2359296 | tf_op jit(solution)/shard_map/reduce_scatter | solution.py:203
  353.9 78.8 %copy-start.46 = (f32[64,2]{0,1:T(2,128)S(1)}, f32[64,2]{0,1:T(2,128)}, u32[]{:S(2)}) copy-start(f32[64,2]{0,1:T(2,128)} %param.29) | copy-start | bytes 1540
  354.0 111.0 %copy-start.19 = (bf16[64,2048]{1,0:T(8,128)(2,1)S(1)}, bf16[64,2048]{1,0:T(8,128)(2,1)}, u32[]{:S(2)}) copy-start(bf16[64,2048]{1,0:T(8,128)(2,1)} %reduce-scatter.5.cloned.1.call-done) | copy-start | bytes 786436
  429.1 35.8 %all-to-all-start.1 = ((bf16[4,2,24,2048]{3,2,1,0:T(8,128)(2,1)}), bf16[4,2,24,2048]{3,2,1,0:T(8,128)(2,1)S(1)}, u32[]{:S(2)}, u32[]{:S(2)}) async-start(bf16[4,2,24,2048]{3,2,1,0:T(8,128)(2,1)} %pad_maximum_fusion.11), calls=%async_computation.5 | async-start | bytes 1572864 | tf_op jit(solution)/shard_map/all_to_all | solution.py:216
  (32 other events, 141.7 us)
Sparse Core Ops, SparseCore 0:
  185.1 36.3 reduce-scatter.4
  237.3 37.4 all-gather.6
  276.5 37.1 all-gather.8
  315.1 28.0 all-gather.4
  345.3 39.7 reduce-scatter.8
  387.3 39.7 reduce-scatter.10
  429.3 35.5 reduce-scatter.6
where the time goes:
time: 480 us; the launch traced here: 474 us
  waiting for transfers between devices  216 us (45%)
  matrix products  141 us (29%)
  local copies, waits for them, and re-layouts  48.5 us (10%)
  other arithmetic  26.4 us (6%)
  blocking collectives  23.7 us (5%)
  between operations  14.7 us (3%)
    reduce_scatter x3, waiting for transfers between devices, hidden_layer(): lax.psum_scatter(partial_rows.astype(jnp.bfloat16), 'tp', scatter_dimensi...  105 us
    dot_general x21, matrix products, product(): return jnp.einsum('...ij,...jk->...ik', left, right, precision=highest)  69.1 us
    all_gather x2, waiting for transfers between devices, gathered(): return lax.all_gather(rows, 'tp', axis=0, tiled=True)  60 us
    reduce_scatter x1, waiting for transfers between devices, body(): lax.psum_scatter(jnp.dot(slab, output_weight, preferred_element_type=jnp....  35.5 us
    dot_general x3, matrix products, hidden_layer(): partial_rows = jnp.dot(hidden, down, preferred_element_type=jnp.float32)  24.7 us
    dot_general x3, matrix products, hidden_layer(): gate_value = jnp.dot(rows, gate, preferred_element_type=jnp.float32)  15.5 us
    all_gather x1, waiting for transfers between devices, body(): everyone = lax.all_gather(normed, 'tp', axis=0, tiled=True)  14.7 us
    unnamed x101, local copies, waits for them, and re-layouts  13.8 us
  transfers between devices with their start and end apart: 8, of which 7 were waited for; matrix products, arithmetic and copies ran while one was open for 9% of the time, Pallas kernels for 0%

commit v1 on v0

v1 whole, which is shorter than its diff:
```python
import functools
import jax
import jax.numpy as jnp
from jax import lax
from jax.experimental import pallas as pl
from jax.experimental.pallas import tpu as pltpu
from jax.sharding import PartitionSpec as P

SPAN = 64
GN_EPS = 0.00064
RMS_EPS = 1e-06
F32, BF16 = jnp.float32, jnp.bfloat16
MESH = pl.DeviceIdType.MESH
NN = (((1,), (0,)), ((), ()))
NT = (((1,), (1,)), ((), ()))
TN = (((0,), (0,)), ((), ()))


def mul(left, right, dims=NN):
    return lax.dot_general(left, right, dims, preferred_element_type=F32)


def halves(x):
    high = x.astype(BF16)
    return high, (x - high.astype(F32)).astype(BF16)


def product(left, right_high, right_low, dims=NN):
    rows = left.shape[0]
    high, low = halves(left)
    both = mul(jnp.concatenate([high, low], axis=0), right_high, dims)
    out = both[:rows] + both[rows:]
    if right_low is not None:
        out = out + mul(high, right_low, dims)
    return out


def mixer_kernel(
    geometry,
    r_ref, k_ref, v_ref, e_ref, dp_ref, spike_ref, gain_ref, w_ref, out_ref,
    local_s, readout_s, maps_s, prefix_s, send_maps, recv_maps,
    mixed_s, part_s, sib_s, summed_s, recv_s,
    map_send, map_recv, sib_send, sib_recv, z_send, z_recv,
):
    n_sp, n_tp, heads = geometry
    n_z = n_tp // 2
    tokens, wide = k_ref.shape
    width = wide // heads
    blocks = tokens // SPAN
    rows = tokens // n_tp
    sp, tp = lax.axis_index("sp"), lax.axis_index("tp")
    z, core = tp // 2, lax.rem(tp, 2)

    barrier = pltpu.get_barrier_semaphore()
    for d in range(1, n_sp):
        pl.semaphore_signal(barrier, inc=1, device_id=(lax.rem(sp + d, n_sp), tp), device_id_type=MESH)
    for d in range(1, n_z):
        pl.semaphore_signal(
            barrier, inc=1, device_id=(sp, lax.rem(z + d, n_z) * 2 + core), device_id_type=MESH
        )
    pl.semaphore_signal(barrier, inc=1, device_id=(sp, z * 2 + 1 - core), device_id_type=MESH)

    def head_mask(shape, dtype):
        first = lax.broadcasted_iota(jnp.int32, shape, 0) // width
        second = lax.broadcasted_iota(jnp.int32, shape, 1) // width
        return (first == second).astype(F32).astype(dtype)

    square = head_mask((wide, wide), BF16)

    def spread(x):
        return jnp.concatenate([x] * heads, axis=0) * square

    def spread_pair(x):
        high, low = halves(x)
        return spread(high), spread(low)

    def gather_heads(x):
        total = x[:width]
        for h in range(1, heads):
            total = total + x[h * width : (h + 1) * width]
        return total

    def lane_of(shape):
        return lax.broadcasted_iota(jnp.int32, shape, 1)

    row_t = lax.broadcasted_iota(jnp.int32, (SPAN, wide), 0)
    col_s = lax.rem(lane_of((SPAN, wide)), SPAN)
    below = row_t > col_s
    above = row_t < col_s
    same = row_t == col_s
    tri = (
        lax.broadcasted_iota(jnp.int32, (SPAN, SPAN), 0)
        >= lax.broadcasted_iota(jnp.int32, (SPAN, SPAN), 1)
    ).astype(F32).astype(BF16)
    tri3 = jnp.concatenate([tri, tri, tri], axis=1)
    eye = same.astype(F32)

    def each_block(b, carry):
        here = pl.ds(pl.multiple_of(b * SPAN, SPAN), SPAN)
        keys = k_ref[here, :].astype(F32)
        square_high, square_low = halves(keys * keys)
        norm = mul(jnp.concatenate([square_high, square_low], axis=0), square)
        norm = norm[:SPAN] + norm[SPAN:]
        unit = keys * lax.rsqrt(norm + 1e-06)
        beta = unit * jax.nn.sigmoid(e_ref[here, :].astype(F32))
        spikes = spike_ref[here, :]
        lane_head = lane_of((SPAN, wide)) // width
        spike = jnp.zeros((SPAN, wide), F32)
        for h in range(heads):
            spike = jnp.where(lane_head == h, spikes[:, h : h + 1], spike)
        decay = -0.6065306597126334 * jax.nn.sigmoid(dp_ref[here, :].astype(F32)) + spike
        decay_1 = decay.astype(BF16)
        rest = decay - decay_1.astype(F32)
        decay_2 = rest.astype(BF16)
        decay_3 = (rest - decay_2.astype(F32)).astype(BF16)
        cumulative = mul(tri3, jnp.concatenate([decay_1, decay_2, decay_3], axis=0))
        total = cumulative[SPAN - 1 : SPAN, :]
        middle = 0.5 * total
        e1 = jnp.exp(cumulative - middle)
        e2 = jnp.exp(cumulative - decay - middle)
        e3 = jnp.exp(middle - cumulative)
        e4 = jnp.exp(middle - cumulative + decay)
        em = jnp.exp(middle)
        et = jnp.exp(total)
        reads = r_ref[here, :].astype(F32)
        values = v_ref[here, :]
        value_wide = spread(values)
        local_sum = jnp.zeros((SPAN, wide), F32)
        for d in range(2):
            strict = below if d == 0 else above
            loose = strict | same
            left_scale, before_scale, right_scale = (e1, e2, e3) if d == 0 else (e4, e3, e2)
            left = jnp.concatenate([unit * before_scale, reads * left_scale], axis=0)
            beta_right = beta * right_scale
            key_right = keys * right_scale
            keep = jnp.concatenate([strict, loose], axis=0)
            from_beta = jnp.where(keep, product(left, *spread_pair(beta_right), dims=NT), 0.0)
            from_key = jnp.where(keep, product(left, *spread_pair(key_right), dims=NT), 0.0)
            key_part = product(from_key, value_wide, None)
            corner_all = from_beta[:SPAN]
            size, inverse = 1, None
            while size < SPAN:
                joined = row_t // (2 * size) == col_s // (2 * size)
                corner = jnp.where(joined & (row_t // size != col_s // size), corner_all, 0.0)
                if size == 1:
                    inverse = eye - corner
                else:
                    pair = spread_pair(inverse)
                    step = product(corner, *pair)
                    inverse = inverse - product(inverse, *spread_pair(step))
                size *= 2
            true_left = left * em
            solved_w = product(inverse, *spread_pair(true_left[:SPAN]))
            solved_v = product(inverse, *spread_pair(-key_part[:SPAN]))
            read = from_beta[SPAN:]
            local_sum = local_sum + key_part[SPAN:] + product(read, *spread_pair(solved_v))
            readout_s[d, here, :] = true_left[SPAN:] - product(read, *spread_pair(solved_w))
            beta_high, beta_low = halves(beta_right * em)
            key_high, key_low = halves(key_right * em)
            w_high, w_low = halves(solved_w)
            v_high, v_low = halves(solved_v)
            beta_three = [beta_high, beta_low, beta_high]
            move = mul(
                jnp.concatenate([w_high, w_high, w_low], axis=0),
                jnp.concatenate(beta_three, axis=0),
                TN,
            )
            put = mul(
                jnp.concatenate([v_high, v_high, v_low, values, values], axis=0),
                jnp.concatenate(beta_three + [key_high, key_low], axis=0),
                TN,
            )
            on_head = lax.broadcasted_iota(jnp.int32, (width, wide), 0) == lax.rem(
                lane_of((width, wide)), width
            )
            wide_mask = square.astype(F32)
            move = gather_heads(move * wide_mask)
            maps_s[d, b, :width, :] = jnp.where(on_head, et, 0.0) - move
            maps_s[d, b, width:, :] = gather_heads(put * wide_mask)
        local_s[here, :] = local_sum
        return carry

    lax.fori_loop(0, blocks, each_block, 0)

    first = (
        lax.broadcasted_iota(jnp.int32, (2 * width, wide), 0)
        == lax.rem(lane_of((2 * width, wide)), width)
    ).astype(F32)
    no_rows = jnp.zeros((width, wide), F32)

    def compose(i, carry):
        new = []
        for d in range(2):
            b = i if d == 0 else blocks - 1 - i
            prefix_s[d, b] = carry[d]
            moved = product(carry[d], *spread_pair(maps_s[d, b, :width, :]))
            new.append(moved + jnp.concatenate([no_rows, maps_s[d, b, width:, :]], axis=0))
        return tuple(new)

    whole = lax.fori_loop(0, blocks, compose, (first, first))
    for d in range(2):
        send_maps[d] = whole[d].astype(BF16)
    pl.semaphore_wait(barrier, n_sp - 1 + n_z)

    copies = []
    for d in range(1, n_sp):
        target = lax.rem(sp + d, n_sp)
        copy = pltpu.make_async_remote_copy(
            src_ref=send_maps.at[(target < sp).astype(jnp.int32)],
            dst_ref=recv_maps.at[sp],
            send_sem=map_send.at[d],
            recv_sem=map_recv.at[sp],
            device_id=(target, tp),
            device_id_type=MESH,
        )
        copy.start()
        copies.append(copy)
    for d in range(1, n_sp):
        source = lax.rem(sp + d, n_sp)
        pltpu.make_async_remote_copy(
            src_ref=send_maps.at[0],
            dst_ref=recv_maps.at[source],
            send_sem=map_send.at[d],
            recv_sem=map_recv.at[source],
            device_id=(source, tp),
            device_id_type=MESH,
        ).wait_recv()
    for copy in copies:
        copy.wait_send()
    recv_maps[sp] = jnp.zeros((2 * width, wide), BF16)

    def enter(i, carry):
        new = []
        for d in range(2):
            k = i if d == 0 else n_sp - 1 - i
            reached = (k < sp) if d == 0 else (k > sp)
            part = recv_maps[k]
            moved = product(carry[d], spread(part[:width]), None) + part[width:].astype(F32)
            new.append(jnp.where(reached, moved, carry[d]))
        return tuple(new)

    entry = lax.fori_loop(0, n_sp, enter, (no_rows, no_rows))

    gain = gain_ref[...].astype(F32)

    def finish(b, carry):
        here = pl.ds(pl.multiple_of(b * SPAN, SPAN), SPAN)
        mix = local_s[here, :]
        for d in range(2):
            start = product(entry[d], *spread_pair(prefix_s[d, b, :width, :]))
            start = start + prefix_s[d, b, width:, :]
            mix = mix + product(readout_s[d, here, :], *spread_pair(start), dims=NT)
        mean = product(mix, square, None) * (1.0 / width)
        mix = mix - mean
        spread_of = product(mix * mix, square, None) * (1.0 / width)
        mixed = mix * lax.rsqrt(spread_of + GN_EPS) * gain
        mixed_s[here, :] = mixed.astype(BF16)
        return carry

    lax.fori_loop(0, blocks, finish, 0)

    sibling = (sp, z * 2 + 1 - core)

    def sib_copy(c):
        return pltpu.make_async_remote_copy(
            src_ref=part_s.at[c, pl.ds(pl.multiple_of((1 - core) * rows, rows), rows), :],
            dst_ref=sib_s.at[c],
            send_sem=sib_send.at[c],
            recv_sem=sib_recv.at[c],
            device_id=sibling,
            device_id_type=MESH,
        )

    def z_copy(c):
        return pltpu.make_async_remote_copy(
            src_ref=summed_s.at[c],
            dst_ref=recv_s.at[z],
            send_sem=z_send.at[c],
            recv_sem=z_recv.at[z],
            device_id=(sp, c * 2 + core),
            device_id_type=MESH,
        )

    def chip_at(i):
        return lax.rem(z + 1 + i, n_z)

    def pass_on(i):
        c = chip_at(i)
        sib_copy(c).wait_recv()
        mine = part_s[c, pl.ds(pl.multiple_of(core * rows, rows), rows), :].astype(F32)
        mine = mine + sib_s[c].astype(F32)
        summed_s[c] = mine.astype(BF16)

        @pl.when(c != z)
        def _():
            z_copy(c).start()

    def project(i, carry):
        c = chip_at(i)
        there = pl.ds(pl.multiple_of(c * (2 * rows), 2 * rows), 2 * rows)
        part_s[c] = mul(mixed_s[there, :], w_ref[...]).astype(BF16)
        sib_copy(c).start()

        @pl.when(i > 0)
        def _():
            pass_on(i - 1)

        return carry

    lax.fori_loop(0, n_z, project, 0)
    pass_on(n_z - 1)
    out_ref[...] = summed_s[z].astype(F32)
    for d in range(1, n_z):
        source = lax.rem(z + d, n_z)
        pltpu.make_async_remote_copy(
            src_ref=summed_s.at[source],
            dst_ref=recv_s.at[source],
            send_sem=z_send.at[source],
            recv_sem=z_recv.at[source],
            device_id=(sp, source * 2 + core),
            device_id_type=MESH,
        ).wait_recv()
        out_ref[...] += recv_s[source].astype(F32)
        z_copy(source).wait_send()
    for c in range(n_z):
        sib_copy(c).wait_send()


def mixer(n_sp, n_tp, receptance, keys, values, erase, decay, spike, gain, weight):
    tokens, wide = keys.shape
    heads = spike.shape[1]
    width = wide // heads
    blocks = tokens // SPAN
    rows = tokens // n_tp
    n_z = n_tp // 2
    model = weight.shape[1]
    vm = pltpu.VMEM
    dma = pltpu.SemaphoreType.DMA
    return pl.pallas_call(
        functools.partial(mixer_kernel, (n_sp, n_tp, heads)),
        out_shape=jax.ShapeDtypeStruct((rows, model), F32),
        in_specs=[pl.BlockSpec(memory_space=vm)] * 8,
        out_specs=pl.BlockSpec(memory_space=vm),
        scratch_shapes=[
            vm((tokens, wide), F32),
            vm((2, tokens, wide), F32),
            vm((2, blocks, 2 * width, wide), F32),
            vm((2, blocks, 2 * width, wide), F32),
            vm((2, 2 * width, wide), BF16),
            vm((n_sp, 2 * width, wide), BF16),
            vm((tokens, wide), BF16),
            vm((n_z, 2 * rows, model), BF16),
            vm((n_z, rows, model), BF16),
            vm((n_z, rows, model), BF16),
            vm((n_z, rows, model), BF16),
            dma((n_sp,)),
            dma((n_sp,)),
            dma((n_z,)),
            dma((n_z,)),
            dma((n_z,)),
            dma((n_z,)),
        ],
        compiler_params=pltpu.CompilerParams(
            collective_id=0, has_side_effects=True, vmem_limit_bytes=56 * 1024 * 1024
        ),
        cost_estimate=pl.CostEstimate(flops=10**10, bytes_accessed=10**7, transcendentals=0),
    )(receptance, keys, values, erase, decay, spike, gain.reshape(1, wide), weight)


highest = lax.Precision.HIGHEST


def body(
    layer_input,
    receptance,
    keys,
    values,
    erase_preact,
    decay_preact,
    decay_spike,
    head_norm_gain,
    output_weight,
    expert_norm_gain,
    routes,
    routing_weight,
    expert_gate_weight,
    expert_up_weight,
    expert_down_weight,
    shared_gate_weight,
    shared_up_weight,
    shared_down_weight,
):
    row_count = layer_input.shape[0]
    model_width = layer_input.shape[1]
    projected = mixer(
        lax.axis_size("sp"), lax.axis_size("tp"), receptance, keys, values, erase_preact,
        decay_preact, decay_spike, head_norm_gain, output_weight,
    )
    residual = layer_input.astype(jnp.float32) + projected
    normed = residual * lax.rsqrt(jnp.mean(residual * residual, axis=-1, keepdims=True) + RMS_EPS)
    normed = (normed * expert_norm_gain.astype(jnp.float32)).astype(jnp.bfloat16)
    everyone = lax.all_gather(normed, "tp", axis=0, tiled=True)
    top_count = routes.shape[1]
    expert_local = expert_gate_weight.shape[0]
    sp_count = lax.axis_size("sp")
    expert_total = expert_local * sp_count
    capacity = max(2, (3 * row_count * top_count + 2 * expert_total - 1) // (2 * expert_total))
    slot_total = sp_count * capacity * expert_local
    entries = routes.reshape(-1)
    entry_count = entries.shape[0]
    expert_hot = (entries[:, None] == lax.broadcasted_iota(jnp.int32, (1, expert_total), 1)).astype(
        jnp.int32
    )
    rank_in = jnp.sum((jnp.cumsum(expert_hot, axis=0) - 1) * expert_hot, axis=1)
    slot_of = entries * capacity + rank_in
    slot_hot = (slot_of[:, None] == lax.broadcasted_iota(jnp.int32, (1, slot_total), 1)).astype(
        jnp.float32
    )
    owner_hot = (
        lax.broadcasted_iota(jnp.int32, (entry_count, 1), 0) // top_count
        == lax.broadcasted_iota(jnp.int32, (1, row_count), 1)
    ).astype(jnp.float32)
    placing = jnp.dot(slot_hot.T, owner_hot, precision=highest)
    weighting = jnp.dot(owner_hot.T, slot_hot * routing_weight.reshape(-1, 1), precision=highest)
    outgoing = jnp.dot(placing.astype(jnp.bfloat16), normed, preferred_element_type=jnp.float32)
    outgoing = outgoing.astype(jnp.bfloat16).reshape(sp_count, expert_local, capacity, model_width)
    arrived = lax.all_to_all(outgoing, "sp", split_axis=0, concat_axis=0, tiled=True)

    def gathered(rows):
        return lax.all_gather(rows, "tp", axis=0, tiled=True)

    def hidden_layer(rows, gate, up, down):
        gate_value = jnp.dot(rows, gate, preferred_element_type=jnp.float32)
        up_value = jnp.dot(rows, up, preferred_element_type=jnp.float32)
        hidden = (jax.nn.silu(gate_value) * up_value).astype(jnp.bfloat16)
        partial_rows = jnp.dot(hidden, down, preferred_element_type=jnp.float32)
        return lax.psum_scatter(
            partial_rows.astype(jnp.bfloat16), "tp", scatter_dimension=0, tiled=True
        )

    shared = hidden_layer(everyone, shared_gate_weight, shared_up_weight, shared_down_weight)
    routed_rows = []
    for j in range(expert_local):
        rows = gathered(arrived[:, j].reshape(sp_count * capacity, model_width))
        out = hidden_layer(
            rows, expert_gate_weight[j], expert_up_weight[j], expert_down_weight[j]
        )
        routed_rows.append(out.reshape(sp_count, 1, capacity, model_width))
    routed_rows = jnp.concatenate(routed_rows, axis=1)
    returned = lax.all_to_all(routed_rows, "sp", split_axis=0, concat_axis=0, tiled=True)
    routed = jnp.dot(
        weighting, returned.reshape(slot_total, model_width).astype(jnp.float32), precision=highest
    )
    return (residual + shared.astype(jnp.float32) + routed).astype(jnp.bfloat16)


def solution(mesh):
    return jax.shard_map(
        body,
        mesh=mesh,
        in_specs=(
            P(("sp", "tp"), None),
            P("sp", "tp"),
            P("sp", "tp"),
            P("sp", "tp"),
            P("sp", "tp"),
            P("sp", "tp"),
            P("sp", "tp"),
            P("tp"),
            P("tp", None),
            P(),
            P(("sp", "tp"), None),
            P(("sp", "tp"), None),
            P("sp", None, "tp"),
            P("sp", None, "tp"),
            P("sp", "tp", None),
            P(None, "tp"),
            P(None, "tp"),
            P("tp", None),
        ),
        out_specs=P(("sp", "tp"), None),
        check_vma=False,
    )
```

time: 480 us -> 357 us (0.74); the launches traced: 474 us -> 357 us
  matrix products: 141 us -> 42.2 us
  Pallas kernels: 0 us -> 87.1 us
  local copies, waits for them, and re-layouts: 48.5 us -> 5.03 us
  waiting for transfers between devices: 216 us -> 185 us
  other arithmetic: 26.4 us -> 4.88 us
  blocking collectives: 23.7 us -> 14.8 us
    dot_general x27 -> x0, matrix products: 97.3 us -> none  [the longest x21 69.1 us: product(): return jnp.einsum('...ij,...jk->...ik', left, right, precision=highest)]
    pallas_call x0 -> x1, Pallas kernels: none -> 87.1 us  [mixer(): pl.pallas_call(functools.partial(mixer_kernel, (n_sp, n_tp, heads)), out_...]
    reduce_scatter x1 -> x0, waiting for transfers between devices: 35.5 us -> none  [body(): lax.psum_scatter(jnp.dot(slab, output_weight, preferred_element_type=jnp....]
    all_gather x1 -> x0, blocking collectives: 11.7 us -> none  [mixer(): lax.all_gather(maps[:, -1].astype(jnp.bfloat16), 'sp').astype(jnp.float32)]
    unnamed x101 -> x15, local copies, waits for them, and re-layouts: 13.8 us -> 2.59 us
    slice x6 -> x0, local copies, waits for them, and re-layouts: 9.58 us -> none  [the longest x1 5.1 us: mixer(): readout = true_left[..., span:, :] - read_solved[..., :width]]
    concatenate x4 -> x0, other arithmetic: 5.42 us -> none  [the longest x2 2.93 us: mixer(): maps = jnp.concatenate([maps[:, :shift], moved], axis=1)]
    transpose x5 -> x0, local copies, waits for them, and re-layouts: 5.21 us -> none  [the longest x4 4.6 us: to_blocks(): jnp.swapaxes(array.reshape(block_count, span, head_number, width), 1, 2)]
  transfers between devices with their start and end apart: 8 -> 7, of which waited for: 7 -> 6; matrix products, arithmetic and copies ran while one was open for 9% -> 12% of each run, Pallas kernels for 0% -> 0%
where the time goes in v1:
time: 357 us
  waiting for transfers between devices  185 us (52%)
  Pallas kernels  87.1 us (24%)
  matrix products  42.2 us (12%)
  blocking collectives  14.8 us (4%)
  between operations  13.6 us (4%)
  local copies, waits for them, and re-layouts  5.03 us (1%)
  other arithmetic  4.88 us (1%)
  starting transfers between devices  4.03 us (1%)
    reduce_scatter x3, waiting for transfers between devices, hidden_layer(): lax.psum_scatter(partial_rows.astype(jnp.bfloat16), 'tp', scatter_dimensi...  106 us
    pallas_call x1, Pallas kernels, mixer(): pl.pallas_call(functools.partial(mixer_kernel, (n_sp, n_tp, heads)), out_...  87.1 us
    all_gather x2, waiting for transfers between devices, gathered(): return lax.all_gather(rows, 'tp', axis=0, tiled=True)  63 us
    dot_general x3, matrix products, hidden_layer(): partial_rows = jnp.dot(hidden, down, preferred_element_type=jnp.float32)  24.5 us
    all_gather x1, waiting for transfers between devices, body(): everyone = lax.all_gather(normed, 'tp', axis=0, tiled=True)  14.9 us
    all_to_all x1, blocking collectives, body(): lax.all_to_all(outgoing, 'sp', split_axis=0, concat_axis=0, tiled=True)  14.8 us
    dot_general x3, matrix products, hidden_layer(): gate_value = jnp.dot(rows, gate, preferred_element_type=jnp.float32)  14.6 us
  transfers between devices with their start and end apart: 7, of which 6 were waited for; matrix products, arithmetic and copies ran while one was open for 12% of the time, Pallas kernels for 0%

profile of v1, /device:TPU:0, one launch (start us, length us, event | category | flops | bytes accessed | tf_op | source)
XLA Modules:
  0.0 356.7 jit_solution(13042062499888559660)
XLA Ops:
  6.5 0.9 copy.23
  8.1 1.6 copy.22.spike_ref
  9.6 1.2 reshape.75.gain_ref
  10.8 87.1 %shard_map.172 = f32[64,2048]{1,0:T(8,128)} custom-call(bf16[512,256]{1,0:T(8,128)(2,1)} %r_ref.1, bf16[512,256]{1,0:T(8,128)(2,1)} %k_ref.1, bf16[512,256]{1,0:T(8,128)(2,1)} %v_ref.1, bf16[512,256]{1,0:T(8,128)(2,1)} %e_ref.1, bf16[512,256]{1,0:T(8,128)(2,1)} %dp_ref.1, f32[512,4]{1,0:T(8,128)} %copy.22.spike_ref, bf16[1,256]{1,0:T(2,128)(2,1)} %reshape.75.gain_ref, ...), custom_call_target="tpu_custom_call" | custom-call | flops 10000000000 | bytes 10000000 | tf_op jit(solution)/shard_map/pallas_call | solution.py:339
  97.9 1.2 multiply_reduce_fusion
  99.5 1.2 multiply_convert_fusion.2
  101.0 14.8 %all_to_all.10 = bf16[4,2,24,2048]{3,2,1,0:T(8,128)(2,1)S(1)} all-to-all(bf16[4,2,24,2048]{3,2,1,0:T(8,128)(2,1)S(1)} %bitcast.50), channel_id=1, replica_groups=mesh['sp'=4,'tp'=8] {'sp'}, dimensions={0} | all-to-all | bytes 1572864 | tf_op jit(solution)/shard_map/all_to_all | solution.py:427
  115.8 1.0 fusion.42
  116.8 0.7 all-gather.8.cloned.1.call-update
  118.3 39.2 %all-gather.6.cloned.1.call-done = bf16[768,2048]{1,0:T(8,128)(2,1)} async-done(((bf16[96,2048]{1,0:T(8,128)(2,1)}), bf16[768,2048]{1,0:T(8,128)(2,1)}) %all-gather.6.cloned.1.call-update) | async-done | bytes 3145744 | tf_op jit(solution)/shard_map/all_gather | solution.py:430
  157.6 5.5 %fusion.9 = f32[768,512]{1,0:T(8,128)} fusion(bf16[768,2048]{1,0:T(8,128)(2,1)} %all-gather.6.cloned.1.call-done, bf16[2,2048,512]{2,1,0:T(8,128)(2,1)} %param.30), kind=kOutput, calls=%fused_computation.14 | convolution fusion | flops 1610612736 | bytes 6815744 | tf_op jit(solution)/shard_map/dot_general | solution.py:433
  163.1 9.3 %convolution_convert_fusion.1 = bf16[768,2048]{1,0:T(8,128)(2,1)} fusion(bf16[2,512,2048]{2,1,0:T(8,128)(2,1)} %param.32, f32[768,512]{1,0:T(8,128)} %fusion.9, bf16[768,2048]{1,0:T(8,128)(2,1)} %all-gather.6.cloned.1.call-done, bf16[2,2048,512]{2,1,0:T(8,128)(2,1)} %param.31), kind=kOutput, calls=%fused_computation.1 | convolution fusion | flops 3225157632 | bytes 12058624 | tf_op jit(solution)/shard_map/dot_general | solution.py:436
  172.6 23.7 %all-gather.8.cloned.1.call-done = bf16[768,2048]{1,0:T(8,128)(2,1)} async-done(((bf16[96,2048]{1,0:T(8,128)(2,1)}), bf16[768,2048]{1,0:T(8,128)(2,1)}) %all-gather.8.cloned.1.call-update) | async-done | bytes 3145744 | tf_op jit(solution)/shard_map/all_gather | solution.py:430
  196.4 5.5 %fusion.4 = f32[768,512]{1,0:T(8,128)} fusion(bf16[768,2048]{1,0:T(8,128)(2,1)} %all-gather.8.cloned.1.call-done, bf16[2,2048,512]{2,1,0:T(8,128)(2,1)} %param.30), kind=kOutput, calls=%fused_computation.9 | convolution fusion | flops 1610612736 | bytes 6815744 | tf_op jit(solution)/shard_map/dot_general | solution.py:433
  201.9 9.2 %convolution_convert_fusion = bf16[768,2048]{1,0:T(8,128)(2,1)} fusion(bf16[2,512,2048]{2,1,0:T(8,128)(2,1)} %param.32, f32[768,512]{1,0:T(8,128)} %fusion.4, bf16[768,2048]{1,0:T(8,128)(2,1)} %all-gather.8.cloned.1.call-done, bf16[2,2048,512]{2,1,0:T(8,128)(2,1)} %param.31), kind=kOutput, calls=%fused_computation | convolution fusion | flops 3225157632 | bytes 12058624 | tf_op jit(solution)/shard_map/dot_general | solution.py:436
  211.2 14.9 %all-gather.4.cloned.1.call-done = bf16[512,2048]{1,0:T(8,128)(2,1)} async-done(((bf16[64,2048]{1,0:T(8,128)(2,1)}), bf16[512,2048]{1,0:T(8,128)(2,1)}) %all-gather.4.cloned.1.call-update) | async-done | bytes 2097168 | tf_op jit(solution)/shard_map/all_gather | solution.py:402
  226.0 3.5 fusion.43
  229.5 6.0 %convolution_convert_fusion.2 = bf16[512,2048]{1,0:T(8,128)(2,1)} fusion(bf16[512,2048]{1,0:T(8,128)(2,1)S(1)} %copy-done, bf16[512,2048]{1,0:T(8,128)(2,1)} %all-gather.4.cloned.1.call-done, bf16[2048,512]{1,0:T(8,128)(2,1)} %param.34, f32[512,512]{1,0:T(8,128)S(1)} %fusion.43), kind=kOutput, calls=%fused_computation.2 | convolution fusion | flops 2150105088 | bytes 9437184 | tf_op jit(solution)/shard_map/dot_general | solution.py:436
  235.6 32.4 %reduce-scatter.6.cloned.1.call-done = bf16[96,2048]{1,0:T(8,128)(2,1)} async-done(((bf16[768,2048]{1,0:T(8,128)(2,1)}), bf16[96,2048]{1,0:T(8,128)(2,1)}) %reduce-scatter.6.cloned.1.call-update) | async-done | bytes 393232 | tf_op jit(solution)/shard_map/reduce_scatter | solution.py:437
  268.0 41.8 %reduce-scatter.8.cloned.1.call-done = bf16[96,2048]{1,0:T(8,128)(2,1)} async-done(((bf16[768,2048]{1,0:T(8,128)(2,1)}), bf16[96,2048]{1,0:T(8,128)(2,1)}) %reduce-scatter.8.cloned.1.call-update) | async-done | bytes 393232 | tf_op jit(solution)/shard_map/reduce_scatter | solution.py:437
  309.8 2.1 pad_maximum_fusion
  311.9 3.6 %all-to-all-start.1 = ((bf16[4,2,24,2048]{3,2,1,0:T(8,128)(2,1)}), bf16[4,2,24,2048]{3,2,1,0:T(8,128)(2,1)S(1)}, u32[]{:S(2)}, u32[]{:S(2)}) async-start(bf16[4,2,24,2048]{3,2,1,0:T(8,128)(2,1)} %pad_maximum_fusion), calls=%async_computation.4 | async-start | bytes 1572864 | tf_op jit(solution)/shard_map/all_to_all | solution.py:450
  316.1 31.4 %reduce-scatter.4.cloned.1.call-done = bf16[64,2048]{1,0:T(8,128)(2,1)} async-done(((bf16[512,2048]{1,0:T(8,128)(2,1)}), bf16[64,2048]{1,0:T(8,128)(2,1)}) %reduce-scatter.4.cloned.1.call-update) | async-done | bytes 262160 | tf_op jit(solution)/shard_map/reduce_scatter | solution.py:437
  347.5 2.3 fusion
  (36 shorter events, 2.9 us)
Async XLA Ops:
  6.5 223.0 %copy-start = (bf16[512,2048]{1,0:T(8,128)(2,1)S(1)}, bf16[512,2048]{1,0:T(8,128)(2,1)}, u32[]{:S(2)}) copy-start(bf16[512,2048]{1,0:T(8,128)(2,1)} %param.35) | copy-start | bytes 6291460
  6.5 151.0 %all-gather.6.cloned.1.call-start = ((), (), s32[]{:S(2)}) async-start(), calls=%async_computation.7 | async-start | bytes 3538944 | tf_op jit(solution)/shard_map/all_gather | solution.py:430
  10.8 87.1 %copy-start.2 = (bf16[64,2048]{1,0:T(8,128)(2,1)S(1)}, bf16[64,2048]{1,0:T(8,128)(2,1)}, u32[]{:S(2)}) copy-start(bf16[64,2048]{1,0:T(8,128)(2,1)} %param.18) | copy-start | bytes 786436
  10.8 88.3 %copy-start.4 = (bf16[2048]{0:T(1024)(128)(2,1)S(1)}, bf16[2048]{0:T(1024)(128)(2,1)}, u32[]{:S(2)}) copy-start(bf16[2048]{0:T(1024)(128)(2,1)} %param.27) | copy-start | bytes 12292
  100.6 16.1 %copy-start.3 = (bf16[64,2048]{1,0:T(8,128)(2,1)}, bf16[64,2048]{1,0:T(8,128)(2,1)S(1)}, u32[]{:S(2)}) copy-start(bf16[64,2048]{1,0:T(8,128)(2,1)S(1)} %multiply_convert_fusion.2) | copy-start | bytes 786436
  116.8 79.6 %all-gather.8.cloned.1.call-start = ((), (), s32[]{:S(2)}) async-start(), calls=%async_computation.9 | async-start | bytes 3538944 | tf_op jit(solution)/shard_map/all_gather | solution.py:430
  117.5 108.5 %all-gather.4.cloned.1.call-start = ((), (), s32[]{:S(2)}) async-start(), calls=%async_computation.5 | async-start | bytes 2359296 | tf_op jit(solution)/shard_map/all_gather | solution.py:402
  118.3 149.7 %reduce-scatter.6.cloned.1.call-start = ((), (), s32[]{:S(2)}) async-start(), calls=%async_computation.8 | async-start | bytes 3538944 | tf_op jit(solution)/shard_map/reduce_scatter | solution.py:437
  172.4 137.4 %reduce-scatter.8.cloned.1.call-start = ((), (), s32[]{:S(2)}) async-start(), calls=%async_computation.10 | async-start | bytes 3538944 | tf_op jit(solution)/shard_map/reduce_scatter | solution.py:437
  211.1 136.4 %reduce-scatter.4.cloned.1.call-start = ((), (), s32[]{:S(2)}) async-start(), calls=%async_computation.6 | async-start | bytes 2359296 | tf_op jit(solution)/shard_map/reduce_scatter | solution.py:437
  235.6 80.0 %copy-start.5 = (f32[64,2]{0,1:T(2,128)S(1)}, f32[64,2]{0,1:T(2,128)}, u32[]{:S(2)}) copy-start(f32[64,2]{0,1:T(2,128)} %param.29) | copy-start | bytes 1540
  235.6 112.0 %copy-start.1 = (f32[64,2048]{1,0:T(8,128)S(1)}, f32[64,2048]{1,0:T(8,128)}, u32[]{:S(2)}) copy-start(f32[64,2048]{1,0:T(8,128)} %shard_map.172) | copy-start | bytes 1572868
  311.9 35.6 %all-to-all-start.1 = ((bf16[4,2,24,2048]{3,2,1,0:T(8,128)(2,1)}), bf16[4,2,24,2048]{3,2,1,0:T(8,128)(2,1)S(1)}, u32[]{:S(2)}, u32[]{:S(2)}) async-start(bf16[4,2,24,2048]{3,2,1,0:T(8,128)(2,1)} %pad_maximum_fusion), calls=%async_computation.4 | async-start | bytes 1572864 | tf_op jit(solution)/shard_map/all_to_all | solution.py:450
Sparse Core Ops, SparseCore 0:
  116.9 40.5 all-gather.5
  159.2 37.1 all-gather.7
  198.0 28.0 all-gather.3
  228.2 39.7 reduce-scatter.5
  270.1 39.6 reduce-scatter.7
  312.0 35.5 reduce-scatter.3

commit v2 on v1

--- a/solution.py
+++ b/solution.py
@@ -1,4 +1,5 @@
 import functools
+import math
 import jax
 import jax.numpy as jnp
 from jax import lax
@@ -7,6 +8,7 @@
 from jax.sharding import PartitionSpec as P
 
 SPAN = 64
+VMEM_LIMIT = 67043328
 GN_EPS = 0.00064
 RMS_EPS = 1e-06
 F32, BF16 = jnp.float32, jnp.bfloat16
@@ -35,14 +37,39 @@
     return out
 
 
+def route_table(routes, weights, experts, capacity, core):
+    rows, top = routes.shape
+    lanes = lax.broadcasted_iota(jnp.int32, (rows, experts), 1)
+    hot = jnp.zeros((rows, experts), F32)
+    weight = jnp.zeros((rows, experts), F32)
+    for j in range(top):
+        chosen = routes[:, j : j + 1] == lanes
+        hot = hot + chosen.astype(F32)
+        weight = weight + jnp.where(chosen, weights[:, j : j + 1], 0.0)
+    row = lax.broadcasted_iota(jnp.int32, (rows, rows), 0)
+    col = lax.broadcasted_iota(jnp.int32, (rows, rows), 1)
+    rank = mul((row > col).astype(F32).astype(BF16), hot.astype(BF16))
+    place = (rank + 1.0 + (core * capacity).astype(F32)) * hot
+    own = lax.broadcasted_iota(jnp.int32, (rows, 2 * rows), 0) + core * rows
+    shifted = (own == lax.broadcasted_iota(jnp.int32, (rows, 2 * rows), 1)).astype(F32).astype(BF16)
+    part_1 = weight.astype(BF16)
+    rest = weight - part_1.astype(F32)
+    part_2 = rest.astype(BF16)
+    part_3 = (rest - part_2.astype(F32)).astype(BF16)
+    placed = mul(place.astype(BF16), shifted, TN)
+    weighed = mul(part_1, shifted, TN) + mul(part_2, shifted, TN) + mul(part_3, shifted, TN)
+    return jnp.concatenate([placed, weighed], axis=0)
+
+
 def mixer_kernel(
     geometry,
-    r_ref, k_ref, v_ref, e_ref, dp_ref, spike_ref, gain_ref, w_ref, out_ref,
+    r_ref, k_ref, v_ref, e_ref, dp_ref, spike_ref, gain_ref, w_ref, routes_ref, rw_ref,
+    out_ref, meta_ref,
     local_s, readout_s, maps_s, prefix_s, send_maps, recv_maps,
     mixed_s, part_s, sib_s, summed_s, recv_s,
-    map_send, map_recv, sib_send, sib_recv, z_send, z_recv,
+    meta_s, meta_send, meta_recv, map_send, map_recv, sib_send, sib_recv, z_send, z_recv,
 ):
-    n_sp, n_tp, heads = geometry
+    n_sp, n_tp, heads, capacity = geometry
     n_z = n_tp // 2
     tokens, wide = k_ref.shape
     width = wide // heads
@@ -54,11 +81,8 @@
     barrier = pltpu.get_barrier_semaphore()
     for d in range(1, n_sp):
         pl.semaphore_signal(barrier, inc=1, device_id=(lax.rem(sp + d, n_sp), tp), device_id_type=MESH)
-    for d in range(1, n_z):
-        pl.semaphore_signal(
-            barrier, inc=1, device_id=(sp, lax.rem(z + d, n_z) * 2 + core), device_id_type=MESH
-        )
-    pl.semaphore_signal(barrier, inc=1, device_id=(sp, z * 2 + 1 - core), device_id_type=MESH)
+    for d in range(1, n_tp):
+        pl.semaphore_signal(barrier, inc=1, device_id=(sp, lax.rem(tp + d, n_tp)), device_id_type=MESH)
 
     def head_mask(shape, dtype):
         first = lax.broadcasted_iota(jnp.int32, shape, 0) // width
@@ -200,7 +224,23 @@
     whole = lax.fori_loop(0, blocks, compose, (first, first))
     for d in range(2):
         send_maps[d] = whole[d].astype(BF16)
-    pl.semaphore_wait(barrier, n_sp - 1 + n_z)
+    pl.semaphore_wait(barrier, n_sp - 1 + n_tp - 1)
+
+    experts = meta_ref.shape[1] // 2
+    meta_s[tp] = route_table(routes_ref[...], rw_ref[...], experts, capacity, core)
+
+    def meta_copy(d):
+        return pltpu.make_async_remote_copy(
+            src_ref=meta_s.at[tp],
+            dst_ref=meta_s.at[tp],
+            send_sem=meta_send.at[d],
+            recv_sem=meta_recv.at[tp],
+            device_id=(sp, lax.rem(tp + d, n_tp)),
+            device_id_type=MESH,
+        )
+
+    for d in range(1, n_tp):
+        meta_copy(d).start()
 
     copies = []
     for d in range(1, n_sp):
@@ -324,9 +364,21 @@
         z_copy(source).wait_send()
     for c in range(n_z):
         sib_copy(c).wait_send()
-
-
-def mixer(n_sp, n_tp, receptance, keys, values, erase, decay, spike, gain, weight):
+    for d in range(1, n_tp):
+        source = lax.rem(tp + d, n_tp)
+        pltpu.make_async_remote_copy(
+            src_ref=meta_s.at[tp],
+            dst_ref=meta_s.at[source],
+            send_sem=meta_send.at[d],
+            recv_sem=meta_recv.at[source],
+            device_id=(sp, source),
+            device_id_type=MESH,
+        ).wait_recv()
+        meta_copy(d).wait_send()
+    meta_ref[...] = meta_s[...]
+
+
+def mixer(n_sp, n_tp, receptance, keys, values, erase, decay, spike, gain, weight, routes, routing, experts, capacity):
     tokens, wide = keys.shape
     heads = spike.shape[1]
     width = wide // heads
@@ -337,10 +389,13 @@
     vm = pltpu.VMEM
     dma = pltpu.SemaphoreType.DMA
     return pl.pallas_call(
-        functools.partial(mixer_kernel, (n_sp, n_tp, heads)),
-        out_shape=jax.ShapeDtypeStruct((rows, model), F32),
-        in_specs=[pl.BlockSpec(memory_space=vm)] * 8,
-        out_specs=pl.BlockSpec(memory_space=vm),
+        functools.partial(mixer_kernel, (n_sp, n_tp, heads, capacity)),
+        out_shape=[
+            jax.ShapeDtypeStruct((rows, model), F32),
+            jax.ShapeDtypeStruct((n_tp, 2 * experts, 2 * rows), F32),
+        ],
+        in_specs=[pl.BlockSpec(memory_space=vm)] * 10,
+        out_specs=[pl.BlockSpec(memory_space=vm)] * 2,
         scratch_shapes=[
             vm((tokens, wide), F32),
             vm((2, tokens, wide), F32),
@@ -353,6 +408,9 @@
             vm((n_z, rows, model), BF16),
             vm((n_z, rows, model), BF16),
             vm((n_z, rows, model), BF16),
+            vm((n_tp, 2 * experts, 2 * rows), F32),
+            dma((n_tp,)),
+            dma((n_tp,)),
             dma((n_sp,)),
             dma((n_sp,)),
             dma((n_z,)),
@@ -364,7 +422,305 @@
             collective_id=0, has_side_effects=True, vmem_limit_bytes=56 * 1024 * 1024
         ),
         cost_estimate=pl.CostEstimate(flops=10**10, bytes_accessed=10**7, transcendentals=0),
-    )(receptance, keys, values, erase, decay, spike, gain.reshape(1, wide), weight)
+    )(receptance, keys, values, erase, decay, spike, gain.reshape(1, wide), weight, routes, routing)
+
+
+def expert_kernel(
+    geometry,
+    input_ref, projected_ref, gain_ref, meta_ref, gate_hbm, up_hbm, down_hbm,
+    shared_gate_hbm, shared_up_hbm, shared_down_hbm, out_ref,
+    gate, up, down, shared_gate, shared_up, shared_down,
+    residual, table, own, xg, sel_out, sel_in, y_buf, y_sib, sh_buf, sh_sib,
+    q_out, q_in, t_out, t_in, fin, fin_sib,
+    w_sem, own_sem, z_send, z_recv, xr_send, xr_recv, sel_send, sel_recv, sr_send, sr_recv,
+    y_send, y_recv, sh_send, sh_recv, q_send, q_recv, t_send, t_recv, fin_sem,
+):
+    n_sp, n_tp, capacity = geometry
+    n_z = n_tp // 2
+    rows, model = input_ref.shape
+    half = model // 2
+    pair = 2 * rows
+    slots = 2 * capacity
+    local = gate_hbm.shape[0]
+    experts = meta_ref.shape[1] // 2
+    hidden = gate_hbm.shape[2]
+    sp, tp = lax.axis_index("sp"), lax.axis_index("tp")
+    z, core = tp // 2, lax.rem(tp, 2)
+    other = 1 - core
+    sibling = (sp, z * 2 + other)
+
+    barrier = pltpu.get_barrier_semaphore()
+    for d in range(1, n_sp):
+        pl.semaphore_signal(barrier, inc=1, device_id=(lax.rem(sp + d, n_sp), tp), device_id_type=MESH)
+    for d in range(1, n_z):
+        pl.semaphore_signal(
+            barrier, inc=1, device_id=(sp, lax.rem(z + d, n_z) * 2 + core), device_id_type=MESH
+        )
+    pl.semaphore_signal(barrier, inc=1, device_id=sibling, device_id_type=MESH)
+
+    loads = [
+        pltpu.make_async_copy(source, target, w_sem.at[i])
+        for i, (source, target) in enumerate(
+            [
+                (gate_hbm, gate), (up_hbm, up), (down_hbm, down), (shared_gate_hbm, shared_gate),
+                (shared_up_hbm, shared_up), (shared_down_hbm, shared_down),
+            ]
+        )
+    ]
+    for load in loads:
+        load.start()
+
+    def remote(source, target, send, recv, device):
+        return pltpu.make_async_remote_copy(
+            src_ref=source, dst_ref=target, send_sem=send, recv_sem=recv,
+            device_id=device, device_id_type=MESH,
+        )
+
+    def rows_at(c):
+        return pl.ds(pl.multiple_of(c * rows, rows), rows)
+
+    total = input_ref[...].astype(F32) + projected_ref[...]
+    residual[...] = total
+    normed = total * lax.rsqrt(jnp.mean(total * total, axis=-1, keepdims=True) + RMS_EPS)
+    normed = (normed * gain_ref[...].astype(F32)).astype(BF16)
+    for h in range(2):
+        own[h] = normed[:, h * half : (h + 1) * half]
+        xg[z, h, rows_at(core), :] = normed[:, h * half : (h + 1) * half]
+    for c in range(n_z):
+        table[c] = meta_ref[2 * c] + meta_ref[2 * c + 1]
+    pl.semaphore_wait(barrier, n_sp - 1 + n_z)
+
+    own_copy = remote(own, xg.at[z, :, rows_at(core), :], own_sem.at[0], own_sem.at[1], sibling)
+    own_copy.start()
+    own_copy.wait_recv()
+
+    def z_copy(c, target):
+        return remote(xg.at[c, core], xg.at[c, core], z_send.at[target], z_recv.at[c], (sp, target * 2 + core))
+
+    for d in range(1, n_z):
+        z_copy(z, lax.rem(z + n_z - d, n_z)).start()
+
+    def relay_x(c):
+        return remote(xg.at[c, core], xg.at[c, core], xr_send.at[c], xr_recv.at[c], sibling)
+
+    def relay_x_in(c):
+        return remote(xg.at[c, other], xg.at[c, other], xr_send.at[c], xr_recv.at[c], sibling)
+
+    def sel_copy(c, g):
+        return remote(
+            sel_out.at[c, g], sel_in.at[c, core, :, sp], sel_send.at[c, g], sel_recv.at[c, sp],
+            (g, tp),
+        )
+
+    def sel_arrival(c, g):
+        return remote(
+            sel_out.at[c, g], sel_in.at[c, core, :, g], sel_send.at[c, g], sel_recv.at[c, g], (g, tp)
+        )
+
+    def relay_sel(c, g):
+        there = sel_in.at[c, core, :, g]
+        return remote(there, there, sr_send.at[c, g], sr_recv.at[c, g], sibling)
+
+    def relay_sel_in(c, g):
+        there = sel_in.at[c, other, :, g]
+        return remote(there, there, sr_send.at[c, g], sr_recv.at[c, g], sibling)
+
+    slot_ids = (lax.broadcasted_iota(jnp.int32, (slots, pair), 0) + 1).astype(F32)
+
+    def picks(c, g):
+        return [(slot_ids == table[c, pl.ds(g * local + j, 1), :]).astype(F32) for j in range(local)]
+
+    def select(c, g, h):
+        chosen = jnp.concatenate(picks(c, g), axis=0).astype(BF16)
+        return mul(chosen, xg[c, h]).astype(BF16).reshape(local, slots, half)
+
+    def send_rows(c):
+        for d in range(1, n_sp):
+            g = lax.rem(sp + d, n_sp)
+            sel_out[c, g] = select(c, g, core)
+            sel_copy(c, g).start()
+
+    send_rows(z)
+    for load in loads:
+        load.wait()
+
+    def feed(x, first, second):
+        gate_value = mul(x[0], first[:half, :]) + mul(x[1], first[half:, :])
+        up_value = mul(x[0], second[:half, :]) + mul(x[1], second[half:, :])
+        return (jax.nn.silu(gate_value) * up_value).astype(BF16)
+
+    def y_copy(c):
+        return remote(y_buf.at[c, other], y_sib.at[c], y_send.at[c], y_recv.at[c], sibling)
+
+    def sh_copy(c):
+        return remote(sh_buf.at[c, other], sh_sib.at[c], sh_send.at[c], sh_recv.at[c], sibling)
+
+    def q_copy(c, g):
+        return remote(q_out.at[c, :, g], q_in.at[c, :, sp], q_send.at[c, g], q_recv.at[c, sp], (g, tp))
+
+    def q_arrival(c, g):
+        return remote(q_out.at[c, :, g], q_in.at[c, :, g], q_send.at[c, g], q_recv.at[c, g], (g, tp))
+
+    def t_copy(c):
+        return remote(t_out.at[c], t_in.at[z], t_send.at[c], t_recv.at[z], (sp, c * 2 + core))
+
+    def t_arrival(c):
+        return remote(t_out.at[c], t_in.at[c], t_send.at[c], t_recv.at[c], (sp, c * 2 + core))
+
+    def combine(c):
+        for d in range(1, n_sp):
+            q_arrival(c, lax.rem(sp + d, n_sp)).wait_recv()
+        result = sh_buf[c, core].astype(F32) + sh_sib[c].astype(F32)
+        for j in range(local):
+            weighted = []
+            for g in range(n_sp):
+                hot = slot_ids == table[c, g * local + j : g * local + j + 1, :]
+                weight = table[c, experts + g * local + j : experts + g * local + j + 1, :]
+                weighted.append(jnp.where(hot, weight, 0.0))
+            high, low = halves(jnp.concatenate(weighted, axis=0))
+            values = q_in[c, j].reshape(n_sp * slots, half)
+            result = result + mul(high, values, TN) + mul(low, values, TN)
+        return result
+
+    def pass_on(c):
+        t_out[c] = combine(c).astype(BF16)
+        t_copy(c).start()
+
+    def step(k, carry):
+        c = lax.rem(z + k, n_z)
+
+        @pl.when(k < n_z - 1)
+        def _():
+            later = lax.rem(z + k + 1, n_z)
+            z_copy(later, z).wait_recv()
+            relay_x(later).start()
+            send_rows(later)
+
+        for d in range(1, n_sp):
+            g = lax.rem(sp + n_sp - d, n_sp)
+            sel_arrival(c, g).wait_recv()
+            relay_sel(c, g).start()
+
+        @pl.when(k > 0)
+        def _():
+            relay_x_in(c).wait_recv()
+
+        for h in range(2):
+            sel_in[c, h, :, sp] = select(c, sp, h)
+        hidden_rows = feed([xg[c, 0], xg[c, 1]], shared_gate, shared_up)
+        for h in range(2):
+            sh_buf[c, h] = mul(hidden_rows, shared_down[:, h * half : (h + 1) * half]).astype(BF16)
+        sh_copy(c).start()
+        for d in range(1, n_sp):
+            relay_sel_in(c, lax.rem(sp + n_sp - d, n_sp)).wait_recv()
+        for j in range(local):
+            x = [sel_in[c, h, j].reshape(n_sp * slots, half) for h in range(2)]
+            hidden_rows = feed(x, gate.at[j], up.at[j])
+            for h in range(2):
+                y = mul(hidden_rows, down[j, :, h * half : (h + 1) * half]).astype(BF16)
+                y_buf[c, h, j] = y.reshape(n_sp, slots, half)
+        y_copy(c).start()
+
+        @pl.when(k > 1)
+        def _():
+            pass_on(lax.rem(z + k - 1, n_z))
+
+        y_copy(c).wait_recv()
+        sh_copy(c).wait_recv()
+        q_out[c] = (y_buf[c, core].astype(F32) + y_sib[c].astype(F32)).astype(BF16)
+        q_in[c, :, sp] = q_out[c, :, sp]
+        for d in range(1, n_sp):
+            q_copy(c, lax.rem(sp + d, n_sp)).start()
+        return carry
+
+    lax.fori_loop(0, n_z, step, 0)
+    pass_on(lax.rem(z + n_z - 1, n_z))
+    fin[...] = combine(z)
+    for d in range(1, n_z):
+        c = lax.rem(z + d, n_z)
+        t_arrival(c).wait_recv()
+        fin[...] += t_in[c].astype(F32)
+    fin_copy = remote(fin.at[rows_at(other), :], fin_sib, fin_sem.at[0], fin_sem.at[1], sibling)
+    fin_copy.start()
+
+    def columns(c):
+        return pl.ds(pl.multiple_of(c * half, half), half)
+
+    mine = residual[:, columns(core)] + fin[rows_at(core), :]
+    out_ref[:, columns(core)] = mine.astype(out_ref.dtype)
+    fin_copy.wait_recv()
+    theirs = residual[:, columns(other)] + fin_sib[...]
+    out_ref[:, columns(other)] = theirs.astype(out_ref.dtype)
+    fin_copy.wait_send()
+    own_copy.wait_send()
+    for c in range(n_z):
+        y_copy(c).wait_send()
+        sh_copy(c).wait_send()
+        for d in range(1, n_sp):
+            g = lax.rem(sp + d, n_sp)
+            sel_copy(c, g).wait_send()
+            relay_sel(c, g).wait_send()
+            q_copy(c, g).wait_send()
+    for d in range(1, n_z):
+        c = lax.rem(z + d, n_z)
+        z_copy(z, c).wait_send()
+        relay_x(c).wait_send()
+        t_copy(c).wait_send()
+
+
+def expert_shapes(n_sp, n_tp, rows, model, local, hidden, experts, capacity):
+    n_z, half, pair, slots = n_tp // 2, model // 2, 2 * rows, 2 * capacity
+    return [
+        ((local, model, hidden), BF16),
+        ((local, model, hidden), BF16),
+        ((local, hidden, model), BF16),
+        ((model, hidden), BF16),
+        ((model, hidden), BF16),
+        ((hidden, model), BF16),
+        ((rows, model), F32),
+        ((n_z, 2 * experts, pair), F32),
+        ((2, rows, half), BF16),
+        ((n_z, 2, pair, half), BF16),
+        ((n_z, n_sp, local, slots, half), BF16),
+        ((n_z, 2, local, n_sp, slots, half), BF16),
+        ((n_z, 2, local, n_sp, slots, half), BF16),
+        ((n_z, local, n_sp, slots, half), BF16),
+        ((n_z, 2, pair, half), BF16),
+        ((n_z, pair, half), BF16),
+        ((n_z, local, n_sp, slots, half), BF16),
+        ((n_z, local, n_sp, slots, half), BF16),
+        ((n_z, pair, half), BF16),
+        ((n_z, pair, half), BF16),
+        ((pair, half), F32),
+        ((rows, half), F32),
+    ]
+
+
+def expert_layer(
+    n_sp, n_tp, shapes, capacity, layer_input, projected, gain, meta, gate, up, down,
+    shared_gate, shared_up, shared_down,
+):
+    n_z = n_tp // 2
+    vm = pltpu.VMEM
+    dma = pltpu.SemaphoreType.DMA
+    inside, outside = pl.BlockSpec(memory_space=vm), pl.BlockSpec(memory_space=pl.ANY)
+    one, two = dma((n_z,)), dma((n_z, n_sp))
+    return pl.pallas_call(
+        functools.partial(expert_kernel, (n_sp, n_tp, capacity)),
+        out_shape=jax.ShapeDtypeStruct(layer_input.shape, BF16),
+        in_specs=[inside] * 4 + [outside] * 6,
+        out_specs=inside,
+        scratch_shapes=[vm(shape, dtype) for shape, dtype in shapes]
+        + [dma((6,)), dma((2,)), one, one, one, one, two, two, two, two]
+        + [one, one, one, one, two, two, one, one, dma((2,))],
+        compiler_params=pltpu.CompilerParams(
+            collective_id=1, has_side_effects=True, vmem_limit_bytes=VMEM_LIMIT
+        ),
+        cost_estimate=pl.CostEstimate(flops=10**10, bytes_accessed=10**7, transcendentals=0),
+    )(
+        layer_input, projected, gain.reshape(1, -1), meta, gate, up, down,
+        shared_gate, shared_up, shared_down,
+    )
 
 
 highest = lax.Precision.HIGHEST
@@ -390,22 +746,32 @@
     shared_up_weight,
     shared_down_weight,
 ):
-    row_count = layer_input.shape[0]
-    model_width = layer_input.shape[1]
-    projected = mixer(
-        lax.axis_size("sp"), lax.axis_size("tp"), receptance, keys, values, erase_preact,
-        decay_preact, decay_spike, head_norm_gain, output_weight,
+    row_count, model_width = layer_input.shape
+    top_count = routes.shape[1]
+    expert_local = expert_gate_weight.shape[0]
+    sp_count, tp_count = lax.axis_size("sp"), lax.axis_size("tp")
+    expert_total = expert_local * sp_count
+    capacity = max(2, (3 * row_count * top_count + 2 * expert_total - 1) // (2 * expert_total))
+    slot_total = sp_count * capacity * expert_local
+    projected, meta = mixer(
+        sp_count, tp_count, receptance, keys, values, erase_preact, decay_preact, decay_spike,
+        head_norm_gain, output_weight, routes, routing_weight, expert_total, capacity,
     )
+    shapes = expert_shapes(
+        sp_count, tp_count, row_count, model_width, expert_local, expert_gate_weight.shape[2],
+        expert_total, capacity,
+    )
+    used = sum(math.prod(shape) * jnp.dtype(dtype).itemsize for shape, dtype in shapes)
+    if used < VMEM_LIMIT * 7 // 8 and (2 * capacity) % 16 == 0:
+        return expert_layer(
+            sp_count, tp_count, shapes, capacity, layer_input, projected, expert_norm_gain, meta,
+            expert_gate_weight, expert_up_weight, expert_down_weight,
+            shared_gate_weight, shared_up_weight, shared_down_weight,
+        )
     residual = layer_input.astype(jnp.float32) + projected
     normed = residual * lax.rsqrt(jnp.mean(residual * residual, axis=-1, keepdims=True) + RMS_EPS)
     normed = (normed * expert_norm_gain.astype(jnp.float32)).astype(jnp.bfloat16)
     everyone = lax.all_gather(normed, "tp", axis=0, tiled=True)
-    top_count = routes.shape[1]
-    expert_local = expert_gate_weight.shape[0]
-    sp_count = lax.axis_size("sp")
-    expert_total = expert_local * sp_count
-    capacity = max(2, (3 * row_count * top_count + 2 * expert_total - 1) // (2 * expert_total))
-    slot_total = sp_count * capacity * expert_local
     entries = routes.reshape(-1)
     entry_count = entries.shape[0]
     expert_hot = (entries[:, None] == lax.broadcasted_iota(jnp.int32, (1, expert_total), 1)).astype(

time: 357 us -> 190 us (0.53)
  waiting for transfers between devices: 185 us -> 0 us
  Pallas kernels: 87.1 us -> 182 us
  matrix products: 42.2 us -> 0 us
  blocking collectives: 14.8 us -> 0 us
  between operations: 13.6 us -> 0.03 us
  other arithmetic: 4.88 us -> 0 us
  starting transfers between devices: 4.03 us -> 0 us
    reduce_scatter x3 -> x0, waiting for transfers between devices: 106 us -> none  [hidden_layer(): lax.psum_scatter(partial_rows.astype(jnp.bfloat16), 'tp', scatter_dimensi...]
    pallas_call x1 -> x2, Pallas kernels: 87.1 us -> 182 us  [the longest x1 94 us: expert_layer(): pl.pallas_call(functools.partial(expert_kernel, (n_sp, n_tp, capacity)),...]
    all_gather x3 -> x0, waiting for transfers between devices: 77.8 us -> none  [the longest x2 63 us: gathered(): return lax.all_gather(rows, 'tp', axis=0, tiled=True)]
    dot_general x10 -> x0, matrix products: 42.2 us -> none  [the longest x3 24.5 us: hidden_layer(): partial_rows = jnp.dot(hidden, down, preferred_element_type=jnp.float32)]
    all_to_all x1 -> x0, blocking collectives: 14.8 us -> none  [body(): lax.all_to_all(outgoing, 'sp', split_axis=0, concat_axis=0, tiled=True)]
    all_to_all x1 -> x0, starting transfers between devices: 3.65 us -> none  [body(): lax.all_to_all(routed_rows, 'sp', split_axis=0, concat_axis=0, tiled=True)]
  transfers between devices with their start and end apart: 7 -> 0, of which waited for: 6 -> 0; matrix products, arithmetic and copies ran while one was open for 12% -> 0% of each run, Pallas kernels for 0% -> 0%
where the time goes in v2:
time: 190 us; the launch traced here: 189 us
  Pallas kernels  182 us (96%)
  local copies, waits for them, and re-layouts  7.8 us (4%)
    pallas_call x1, Pallas kernels, expert_layer(): pl.pallas_call(functools.partial(expert_kernel, (n_sp, n_tp, capacity)),...  94 us
    pallas_call x1, Pallas kernels, mixer(): pl.pallas_call(functools.partial(mixer_kernel, (n_sp, n_tp, heads, capaci...  87.6 us
    unnamed x6, local copies, waits for them, and re-layouts  5.96 us

profile of v2, /device:TPU:0, one launch (start us, length us, event | category | flops | bytes accessed | tf_op | source)
XLA Modules:
  0.0 189.4 jit_solution(5846017594893150196)
XLA Ops:
  0.0 1.5 copy.19.spike_ref
  1.6 1.4 copy.20.routes_ref
  2.9 1.4 copy.21.rw_ref
  4.3 1.2 reshape.6.gain_ref
  5.5 0.0 copy-start
  5.5 87.6 %shard_map.172 = (f32[64,2048]{1,0:T(8,128)}, f32[8,16,128]{2,1,0:T(8,128)}) custom-call(bf16[512,256]{1,0:T(8,128)(2,1)} %r_ref.1, bf16[512,256]{1,0:T(8,128)(2,1)} %k_ref.1, bf16[512,256]{1,0:T(8,128)(2,1)} %v_ref.1, bf16[512,256]{1,0:T(8,128)(2,1)} %e_ref.1, bf16[512,256]{1,0:T(8,128)(2,1)} %dp_ref.1, f32[512,4]{1,0:T(8,128)} %copy.19.spike_ref, ...), custom_call_target="tpu_custom_call" | custom-call | flops 10000000000 | bytes 10000000 | tf_op jit(solution)/shard_map/pallas_call | solution.py:391
  93.1 0.0 copy-done
  93.1 0.6 reshape.7.gain_ref
  93.7 94.0 %shard_map.173 = bf16[64,2048]{1,0:T(8,128)(2,1)} custom-call(bf16[64,2048]{1,0:T(8,128)(2,1)} %input_ref.1, f32[64,2048]{1,0:T(8,128)} %get-tuple-element.7.projected_ref, bf16[1,2048]{1,0:T(2,128)(2,1)} %reshape.7.gain_ref, f32[8,16,128]{2,1,0:T(8,128)} %get-tuple-element.8.meta_ref, bf16[2,2048,512]{2,1,0:T(8,128)(2,1)} %gate_hbm.1, ...), custom_call_target="tpu_custom_call" | custom-call | flops 10000000000 | bytes 10000000 | tf_op jit(solution)/shard_map/pallas_call | solution.py:708
  187.7 1.7 copy.23
Async XLA Ops:
  5.5 87.6 %copy-start = (bf16[2048]{0:T(1024)(128)(2,1)S(1)}, bf16[2048]{0:T(1024)(128)(2,1)}, u32[]{:S(2)}) copy-start(bf16[2048]{0:T(1024)(128)(2,1)} %param.27) | copy-start | bytes 12292

commit v3 on v2

--- a/solution.py
+++ b/solution.py
@@ -8,6 +8,7 @@
 from jax.sharding import PartitionSpec as P
 
 SPAN = 64
+TOGETHER = 4
 VMEM_LIMIT = 67043328
 GN_EPS = 0.00064
 RMS_EPS = 1e-06
@@ -27,6 +28,13 @@
     return high, (x - high.astype(F32)).astype(BF16)
 
 
+def thirds(x):
+    first = x.astype(BF16)
+    rest = x - first.astype(F32)
+    second = rest.astype(BF16)
+    return first, second, (rest - second.astype(F32)).astype(BF16)
+
+
 def product(left, right_high, right_low, dims=NN):
     rows = left.shape[0]
     high, low = halves(left)
@@ -38,26 +46,22 @@
 
 
 def route_table(routes, weights, experts, capacity, core):
-    rows, top = routes.shape
-    lanes = lax.broadcasted_iota(jnp.int32, (rows, experts), 1)
-    hot = jnp.zeros((rows, experts), F32)
-    weight = jnp.zeros((rows, experts), F32)
+    top, rows = routes.shape
+    lines = lax.broadcasted_iota(jnp.int32, (experts, rows), 0)
+    hot = jnp.zeros((experts, rows), F32)
+    weight = jnp.zeros((experts, rows), F32)
     for j in range(top):
-        chosen = routes[:, j : j + 1] == lanes
+        chosen = routes[j : j + 1, :] == lines
         hot = hot + chosen.astype(F32)
-        weight = weight + jnp.where(chosen, weights[:, j : j + 1], 0.0)
+        weight = weight + jnp.where(chosen, weights[j : j + 1, :], 0.0)
     row = lax.broadcasted_iota(jnp.int32, (rows, rows), 0)
     col = lax.broadcasted_iota(jnp.int32, (rows, rows), 1)
-    rank = mul((row > col).astype(F32).astype(BF16), hot.astype(BF16))
+    rank = mul(hot.astype(BF16), (row < col).astype(F32).astype(BF16))
     place = (rank + 1.0 + (core * capacity).astype(F32)) * hot
     own = lax.broadcasted_iota(jnp.int32, (rows, 2 * rows), 0) + core * rows
     shifted = (own == lax.broadcasted_iota(jnp.int32, (rows, 2 * rows), 1)).astype(F32).astype(BF16)
-    part_1 = weight.astype(BF16)
-    rest = weight - part_1.astype(F32)
-    part_2 = rest.astype(BF16)
-    part_3 = (rest - part_2.astype(F32)).astype(BF16)
-    placed = mul(place.astype(BF16), shifted, TN)
-    weighed = mul(part_1, shifted, TN) + mul(part_2, shifted, TN) + mul(part_3, shifted, TN)
+    placed = mul(place.astype(BF16), shifted)
+    weighed = sum(mul(part, shifted) for part in thirds(weight))
     return jnp.concatenate([placed, weighed], axis=0)
 
 
@@ -65,7 +69,7 @@
     geometry,
     r_ref, k_ref, v_ref, e_ref, dp_ref, spike_ref, gain_ref, w_ref, routes_ref, rw_ref,
     out_ref, meta_ref,
-    local_s, readout_s, maps_s, prefix_s, send_maps, recv_maps,
+    spike_s, local_s, readout_s, maps_s, prefix_s, send_maps, recv_maps,
     mixed_s, part_s, sib_s, summed_s, recv_s,
     meta_s, meta_send, meta_recv, map_send, map_recv, sib_send, sib_recv, z_send, z_recv,
 ):
@@ -119,70 +123,82 @@
     tri3 = jnp.concatenate([tri, tri, tri], axis=1)
     eye = same.astype(F32)
 
-    def each_block(b, carry):
-        here = pl.ds(pl.multiple_of(b * SPAN, SPAN), SPAN)
-        keys = k_ref[here, :].astype(F32)
-        square_high, square_low = halves(keys * keys)
-        norm = mul(jnp.concatenate([square_high, square_low], axis=0), square)
-        norm = norm[:SPAN] + norm[SPAN:]
-        unit = keys * lax.rsqrt(norm + 1e-06)
-        beta = unit * jax.nn.sigmoid(e_ref[here, :].astype(F32))
-        spikes = spike_ref[here, :]
-        lane_head = lane_of((SPAN, wide)) // width
-        spike = jnp.zeros((SPAN, wide), F32)
-        for h in range(heads):
-            spike = jnp.where(lane_head == h, spikes[:, h : h + 1], spike)
-        decay = -0.6065306597126334 * jax.nn.sigmoid(dp_ref[here, :].astype(F32)) + spike
-        decay_1 = decay.astype(BF16)
-        rest = decay - decay_1.astype(F32)
-        decay_2 = rest.astype(BF16)
-        decay_3 = (rest - decay_2.astype(F32)).astype(BF16)
-        cumulative = mul(tri3, jnp.concatenate([decay_1, decay_2, decay_3], axis=0))
-        total = cumulative[SPAN - 1 : SPAN, :]
-        middle = 0.5 * total
-        e1 = jnp.exp(cumulative - middle)
-        e2 = jnp.exp(cumulative - decay - middle)
-        e3 = jnp.exp(middle - cumulative)
-        e4 = jnp.exp(middle - cumulative + decay)
-        em = jnp.exp(middle)
-        et = jnp.exp(total)
-        reads = r_ref[here, :].astype(F32)
-        values = v_ref[here, :]
-        value_wide = spread(values)
-        local_sum = jnp.zeros((SPAN, wide), F32)
-        for d in range(2):
-            strict = below if d == 0 else above
-            loose = strict | same
-            left_scale, before_scale, right_scale = (e1, e2, e3) if d == 0 else (e4, e3, e2)
-            left = jnp.concatenate([unit * before_scale, reads * left_scale], axis=0)
-            beta_right = beta * right_scale
-            key_right = keys * right_scale
-            keep = jnp.concatenate([strict, loose], axis=0)
-            from_beta = jnp.where(keep, product(left, *spread_pair(beta_right), dims=NT), 0.0)
-            from_key = jnp.where(keep, product(left, *spread_pair(key_right), dims=NT), 0.0)
-            key_part = product(from_key, value_wide, None)
-            corner_all = from_beta[:SPAN]
-            size, inverse = 1, None
-            while size < SPAN:
-                joined = row_t // (2 * size) == col_s // (2 * size)
-                corner = jnp.where(joined & (row_t // size != col_s // size), corner_all, 0.0)
-                if size == 1:
-                    inverse = eye - corner
-                else:
-                    pair = spread_pair(inverse)
-                    step = product(corner, *pair)
-                    inverse = inverse - product(inverse, *spread_pair(step))
-                size *= 2
-            true_left = left * em
-            solved_w = product(inverse, *spread_pair(true_left[:SPAN]))
-            solved_v = product(inverse, *spread_pair(-key_part[:SPAN]))
-            read = from_beta[SPAN:]
-            local_sum = local_sum + key_part[SPAN:] + product(read, *spread_pair(solved_v))
-            readout_s[d, here, :] = true_left[SPAN:] - product(read, *spread_pair(solved_w))
+    def product_all(lefts, rights, dims=NN):
+        pairs = [spread_pair(right) for right in rights]
+        return [product(left, *pair, dims=dims) for left, pair in zip(lefts, pairs)]
+
+    def each_group(i, carry):
+        chains = []
+        blocks_here = []
+        for b in [i * TOGETHER + n for n in range(TOGETHER)]:
+            here = pl.ds(pl.multiple_of(b * SPAN, SPAN), SPAN)
+            keys = k_ref[here, :].astype(F32)
+            square_high, square_low = halves(keys * keys)
+            norm = mul(jnp.concatenate([square_high, square_low], axis=0), square)
+            norm = norm[:SPAN] + norm[SPAN:]
+            unit = keys * lax.rsqrt(norm + 1e-06)
+            beta = unit * jax.nn.sigmoid(e_ref[here, :].astype(F32))
+            decay = -0.6065306597126334 * jax.nn.sigmoid(dp_ref[here, :].astype(F32))
+            decay = decay + spike_s[here, :]
+            decay_1, decay_2, decay_3 = thirds(decay)
+            cumulative = mul(tri3, jnp.concatenate([decay_1, decay_2, decay_3], axis=0))
+            total = cumulative[SPAN - 1 : SPAN, :]
+            middle = 0.5 * total
+            e1 = jnp.exp(cumulative - middle)
+            e2 = jnp.exp(cumulative - decay - middle)
+            e3 = jnp.exp(middle - cumulative)
+            e4 = jnp.exp(middle - cumulative + decay)
+            em = jnp.exp(middle)
+            et = jnp.exp(total)
+            reads = r_ref[here, :].astype(F32)
+            values = v_ref[here, :]
+            value_wide = spread(values)
+            blocks_here.append((b, here))
+            for d in range(2):
+                left_scale, before_scale, right_scale = (e1, e2, e3) if d == 0 else (e4, e3, e2)
+                left = jnp.concatenate([unit * before_scale, reads * left_scale], axis=0)
+                chains.append(
+                    (d, b, here, left, beta * right_scale, keys * right_scale, em, et, values, value_wide)
+                )
+        lefts = [c[3] for c in chains]
+        keeps = []
+        for c in chains:
+            strict = below if c[0] == 0 else above
+            keeps.append(jnp.concatenate([strict, strict | same], axis=0))
+        from_beta = product_all(lefts, [c[4] for c in chains], NT)
+        from_beta = [jnp.where(keep, x, 0.0) for keep, x in zip(keeps, from_beta)]
+        from_key = product_all(lefts, [c[5] for c in chains], NT)
+        from_key = [jnp.where(keep, x, 0.0) for keep, x in zip(keeps, from_key)]
+        key_part = [product(x, c[9], None) for x, c in zip(from_key, chains)]
+        size, inverse = 1, None
+        while size < SPAN:
+            corner_mask = (row_t // (2 * size) == col_s // (2 * size)) & (row_t // size != col_s // size)
+            corner = [jnp.where(corner_mask, x[:SPAN], 0.0) for x in from_beta]
+            if size == 1:
+                inverse = [eye - x for x in corner]
+            else:
+                steps = product_all(corner, inverse)
+                steps = product_all(inverse, steps)
+                inverse = [x - y for x, y in zip(inverse, steps)]
+            size *= 2
+        true_left = [c[3] * c[6] for c in chains]
+        solved_w = product_all(inverse, [x[:SPAN] for x in true_left])
+        solved_v = product_all(inverse, [-x[:SPAN] for x in key_part])
+        read = [x[SPAN:] for x in from_beta]
+        read_v = product_all(read, solved_v)
+        read_w = product_all(read, solved_w)
+        on_head = lax.broadcasted_iota(jnp.int32, (width, wide), 0) == lax.rem(
+            lane_of((width, wide)), width
+        )
+        wide_mask = square.astype(F32)
+        locals_now = []
+        for n, (d, b, here, left, beta_right, key_right, em, et, values, value_wide) in enumerate(chains):
+            locals_now.append(key_part[n][SPAN:] + read_v[n])
+            readout_s[d, here, :] = true_left[n][SPAN:] - read_w[n]
             beta_high, beta_low = halves(beta_right * em)
             key_high, key_low = halves(key_right * em)
-            w_high, w_low = halves(solved_w)
-            v_high, v_low = halves(solved_v)
+            w_high, w_low = halves(solved_w[n])
+            v_high, v_low = halves(solved_v[n])
             beta_three = [beta_high, beta_low, beta_high]
             move = mul(
                 jnp.concatenate([w_high, w_high, w_low], axis=0),
@@ -194,17 +210,18 @@
                 jnp.concatenate(beta_three + [key_high, key_low], axis=0),
                 TN,
             )
-            on_head = lax.broadcasted_iota(jnp.int32, (width, wide), 0) == lax.rem(
-                lane_of((width, wide)), width
-            )
-            wide_mask = square.astype(F32)
             move = gather_heads(move * wide_mask)
             maps_s[d, b, :width, :] = jnp.where(on_head, et, 0.0) - move
             maps_s[d, b, width:, :] = gather_heads(put * wide_mask)
-        local_s[here, :] = local_sum
+        for n, (b, here) in enumerate(blocks_here):
+            local_s[here, :] = locals_now[2 * n] + locals_now[2 * n + 1]
         return carry
 
-    lax.fori_loop(0, blocks, each_block, 0)
+    head_row = lax.broadcasted_iota(jnp.int32, (heads, wide), 0)
+    head_hot = (head_row == lane_of((heads, wide)) // width).astype(F32).astype(BF16)
+    spike_s[...] = sum(mul(part, head_hot, TN) for part in thirds(spike_ref[...]))
+
+    lax.fori_loop(0, blocks // TOGETHER, each_group, 0)
 
     first = (
         lax.broadcasted_iota(jnp.int32, (2 * width, wide), 0)
@@ -281,7 +298,7 @@
 
     entry = lax.fori_loop(0, n_sp, enter, (no_rows, no_rows))
 
-    gain = gain_ref[...].astype(F32)
+    gain = gain_ref[...].astype(F32).reshape(1, wide)
 
     def finish(b, carry):
         here = pl.ds(pl.multiple_of(b * SPAN, SPAN), SPAN)
@@ -297,8 +314,6 @@
         mixed_s[here, :] = mixed.astype(BF16)
         return carry
 
-    lax.fori_loop(0, blocks, finish, 0)
-
     sibling = (sp, z * 2 + 1 - core)
 
     def sib_copy(c):
@@ -338,6 +353,8 @@
     def project(i, carry):
         c = chip_at(i)
         there = pl.ds(pl.multiple_of(c * (2 * rows), 2 * rows), 2 * rows)
+        first_block = c * (2 * rows // SPAN)
+        lax.fori_loop(first_block, first_block + 2 * rows // SPAN, finish, 0)
         part_s[c] = mul(mixed_s[there, :], w_ref[...]).astype(BF16)
         sib_copy(c).start()
 
@@ -398,6 +415,7 @@
         out_specs=[pl.BlockSpec(memory_space=vm)] * 2,
         scratch_shapes=[
             vm((tokens, wide), F32),
+            vm((tokens, wide), F32),
             vm((2, tokens, wide), F32),
             vm((2, blocks, 2 * width, wide), F32),
             vm((2, blocks, 2 * width, wide), F32),
@@ -422,7 +440,7 @@
             collective_id=0, has_side_effects=True, vmem_limit_bytes=56 * 1024 * 1024
         ),
         cost_estimate=pl.CostEstimate(flops=10**10, bytes_accessed=10**7, transcendentals=0),
-    )(receptance, keys, values, erase, decay, spike, gain.reshape(1, wide), weight, routes, routing)
+    )(receptance, keys, values, erase, decay, spike.T, gain, weight, routes.T, routing.T)
 
 
 def expert_kernel(
@@ -482,7 +500,7 @@
     total = input_ref[...].astype(F32) + projected_ref[...]
     residual[...] = total
     normed = total * lax.rsqrt(jnp.mean(total * total, axis=-1, keepdims=True) + RMS_EPS)
-    normed = (normed * gain_ref[...].astype(F32)).astype(BF16)
+    normed = (normed * gain_ref[...].astype(F32).reshape(1, model)).astype(BF16)
     for h in range(2):
         own[h] = normed[:, h * half : (h + 1) * half]
         xg[z, h, rows_at(core), :] = normed[:, h * half : (h + 1) * half]
@@ -718,7 +736,7 @@
         ),
         cost_estimate=pl.CostEstimate(flops=10**10, bytes_accessed=10**7, transcendentals=0),
     )(
-        layer_input, projected, gain.reshape(1, -1), meta, gate, up, down,
+        layer_input, projected, gain, meta, gate, up, down,
         shared_gate, shared_up, shared_down,
     )
 

time: 190 us -> 151 us (0.79)
  Pallas kernels: 182 us -> 149 us
  local copies, waits for them, and re-layouts: 7.8 us -> 1.67 us
    pallas_call x1, Pallas kernels: 87.6 us -> 55 us  [mixer(): pl.pallas_call(functools.partial(mixer_kernel, (n_sp, n_tp, heads, capaci...]
    unnamed x6 -> x1, local copies, waits for them, and re-layouts: 5.96 us -> 1.67 us
where the time goes in v3:
time: 151 us
  Pallas kernels  149 us (99%)
  local copies, waits for them, and re-layouts  1.67 us (1%)
    pallas_call x1, Pallas kernels, expert_layer(): pl.pallas_call(functools.partial(expert_kernel, (n_sp, n_tp, capacity)),...  93.9 us
    pallas_call x1, Pallas kernels, mixer(): pl.pallas_call(functools.partial(mixer_kernel, (n_sp, n_tp, heads, capaci...  55 us

profile of v3, /device:TPU:0, one launch (start us, length us, event | category | flops | bytes accessed | tf_op | source)
XLA Modules:
  0.0 150.6 jit_solution(7410597705447908731)
XLA Ops:
  0.0 55.0 %shard_map.172 = (f32[64,2048]{1,0:T(8,128)}, f32[8,16,128]{2,1,0:T(8,128)}) custom-call(bf16[512,256]{1,0:T(8,128)(2,1)} %r_ref.1, bf16[512,256]{1,0:T(8,128)(2,1)} %k_ref.1, bf16[512,256]{1,0:T(8,128)(2,1)} %v_ref.1, bf16[512,256]{1,0:T(8,128)(2,1)} %e_ref.1, bf16[512,256]{1,0:T(8,128)(2,1)} %dp_ref.1, f32[4,512]{1,0:T(4,128)} %bitcast.3, ...), custom_call_target="tpu_custom_call" | custom-call | flops 10000000000 | bytes 10000000 | tf_op jit(solution)/shard_map/pallas_call | solution.py:408
  55.0 93.9 %shard_map.173 = bf16[64,2048]{1,0:T(8,128)(2,1)} custom-call(bf16[64,2048]{1,0:T(8,128)(2,1)} %input_ref.1, f32[64,2048]{1,0:T(8,128)} %get-tuple-element.7.projected_ref, bf16[2048]{0:T(1024)(128)(2,1)} %gain_ref.3, f32[8,16,128]{2,1,0:T(8,128)} %get-tuple-element.8.meta_ref, bf16[2,2048,512]{2,1,0:T(8,128)(2,1)} %gate_hbm.1, ...), custom_call_target="tpu_custom_call" | custom-call | flops 10000000000 | bytes 10000000 | tf_op jit(solution)/shard_map/pallas_call | solution.py:726
  148.9 1.7 %copy.20 = bf16[64,2048]{1,0:T(8,128)(2,1)} copy(bf16[64,2048]{1,0:T(8,128)(2,1)} %shard_map.173) | data formatting | bytes 524288

commit v4 on v3

--- a/solution.py
+++ b/solution.py
@@ -43,6 +43,34 @@
     if right_low is not None:
         out = out + mul(high, right_low, dims)
     return out
+
+
+def near_order(n_z):
+    table = []
+    for z in range(n_z):
+        others = sorted((c for c in range(n_z) if c != z), key=lambda c: (abs(c - z), c))
+        table.append(others + [z])
+    return table
+
+
+def out_order(n_z):
+    return [line[1:-1] + line[:1] + line[-1:] for line in near_order(n_z)]
+
+
+def far_order(n_z):
+    table = []
+    for z in range(n_z):
+        others = sorted((c for c in range(n_z) if c != z), key=lambda c: (-abs(c - z), c))
+        table.append(others + [z])
+    return table
+
+
+def pick(table, z, k):
+    found = jnp.int32(0)
+    for i, line in enumerate(table):
+        for j, value in enumerate(line):
+            found = found + value * ((z == i) & (k == j)).astype(jnp.int32)
+    return found
 
 
 def route_table(routes, weights, experts, capacity, core):
@@ -326,18 +354,41 @@
             device_id_type=MESH,
         )
 
+    low_end = ((z == 0) & (n_z > 2)).astype(jnp.int32)
+    high_end = ((z == n_z - 1) & (n_z > 2)).astype(jnp.int32)
+    at_end = low_end + high_end
+    inner = low_end + high_end * (n_z - 2)
+
     def z_copy(c):
+        through = at_end * (c != inner).astype(jnp.int32)
+        slot = through * (n_z + c) + (1 - through) * z
+        target = at_end * inner + (1 - at_end) * c
         return pltpu.make_async_remote_copy(
             src_ref=summed_s.at[c],
-            dst_ref=recv_s.at[z],
+            dst_ref=recv_s.at[slot],
             send_sem=z_send.at[c],
-            recv_sem=z_recv.at[z],
-            device_id=(sp, c * 2 + core),
+            recv_sem=z_recv.at[slot],
+            device_id=(sp, target * 2 + core),
             device_id_type=MESH,
         )
 
+    def arrival(slot):
+        return pltpu.make_async_remote_copy(
+            src_ref=summed_s.at[0],
+            dst_ref=recv_s.at[slot],
+            send_sem=z_send.at[0],
+            recv_sem=z_recv.at[slot],
+            device_id=sibling,
+            device_id_type=MESH,
+        )
+
+    def joins(c):
+        return (n_z > 2) & (((z == 1) & (c > 1)) | ((z == n_z - 2) & (c < n_z - 2)))
+
+    far = far_order(n_z)
+
     def chip_at(i):
-        return lax.rem(z + 1 + i, n_z)
+        return pick(far, z, i)
 
     def pass_on(i):
         c = chip_at(i)
@@ -346,7 +397,7 @@
         mine = mine + sib_s[c].astype(F32)
         summed_s[c] = mine.astype(BF16)
 
-        @pl.when(c != z)
+        @pl.when((c != z) & jnp.logical_not(joins(c)))
         def _():
             z_copy(c).start()
 
@@ -366,19 +417,30 @@
 
     lax.fori_loop(0, n_z, project, 0)
     pass_on(n_z - 1)
+    for i in range(n_z - 1):
+        c = chip_at(i)
+
+        @pl.when(joins(c))
+        def _():
+            arrival(n_z + c).wait_recv()
+            summed_s[c] = (summed_s[c].astype(F32) + recv_s[n_z + c].astype(F32)).astype(BF16)
+            z_copy(c).start()
+
     out_ref[...] = summed_s[z].astype(F32)
+    for source in range(n_z):
+        direct = z != source
+        if n_z > 2 and source == 0:
+            direct = z == 1
+        if n_z > 2 and source == n_z - 1:
+            direct = z == n_z - 2
+
+        @pl.when(direct)
+        def _():
+            arrival(source).wait_recv()
+            out_ref[...] += recv_s[source].astype(F32)
+
     for d in range(1, n_z):
-        source = lax.rem(z + d, n_z)
-        pltpu.make_async_remote_copy(
-            src_ref=summed_s.at[source],
-            dst_ref=recv_s.at[source],
-            send_sem=z_send.at[source],
-            recv_sem=z_recv.at[source],
-            device_id=(sp, source * 2 + core),
-            device_id_type=MESH,
-        ).wait_recv()
-        out_ref[...] += recv_s[source].astype(F32)
-        z_copy(source).wait_send()
+        z_copy(lax.rem(z + d, n_z)).wait_send()
     for c in range(n_z):
         sib_copy(c).wait_send()
     for d in range(1, n_tp):
@@ -425,7 +487,7 @@
             vm((n_z, 2 * rows, model), BF16),
             vm((n_z, rows, model), BF16),
             vm((n_z, rows, model), BF16),
-            vm((n_z, rows, model), BF16),
+            vm((2 * n_z, rows, model), BF16),
             vm((n_tp, 2 * experts, 2 * rows), F32),
             dma((n_tp,)),
             dma((n_tp,)),
@@ -434,7 +496,7 @@
             dma((n_z,)),
             dma((n_z,)),
             dma((n_z,)),
-            dma((n_z,)),
+            dma((2 * n_z,)),
         ],
         compiler_params=pltpu.CompilerParams(
             collective_id=0, has_side_effects=True, vmem_limit_bytes=56 * 1024 * 1024
@@ -512,11 +574,27 @@
     own_copy.start()
     own_copy.wait_recv()
 
-    def z_copy(c, target):
-        return remote(xg.at[c, core], xg.at[c, core], z_send.at[target], z_recv.at[c], (sp, target * 2 + core))
-
-    for d in range(1, n_z):
-        z_copy(z, lax.rem(z + n_z - d, n_z)).start()
+    def up_copy(c):
+        there = xg.at[c, core]
+        return remote(there, there, z_send.at[0, c], z_recv.at[c], (sp, lax.rem(z + 1, n_z) * 2 + core))
+
+    def down_copy(c):
+        there = xg.at[c, core]
+        return remote(
+            there, there, z_send.at[1, c], z_recv.at[c], (sp, lax.rem(z + n_z - 1, n_z) * 2 + core)
+        )
+
+    def along(c, act):
+        @pl.when((c <= z) & (z < n_z - 1))
+        def _():
+            act(up_copy(c))
+
+        @pl.when((c >= z) & (z > 0))
+        def _():
+            act(down_copy(c))
+
+    near = near_order(n_z)
+    along(z, lambda copy: copy.start())
 
     def relay_x(c):
         return remote(xg.at[c, core], xg.at[c, core], xr_send.at[c], xr_recv.at[c], sibling)
@@ -559,6 +637,16 @@
             sel_copy(c, g).start()
 
     send_rows(z)
+
+    def take(k, carry):
+        c = pick(near, z, k)
+        up_copy(c).wait_recv()
+        along(c, lambda copy: copy.start())
+        relay_x(c).start()
+        send_rows(c)
+        return carry
+
+    lax.fori_loop(0, n_z - 1, take, 0)
     for load in loads:
         load.wait()
 
@@ -604,22 +692,17 @@
         t_out[c] = combine(c).astype(BF16)
         t_copy(c).start()
 
+    out = out_order(n_z)
+
     def step(k, carry):
-        c = lax.rem(z + k, n_z)
-
-        @pl.when(k < n_z - 1)
-        def _():
-            later = lax.rem(z + k + 1, n_z)
-            z_copy(later, z).wait_recv()
-            relay_x(later).start()
-            send_rows(later)
+        c = pick(out, z, k)
 
         for d in range(1, n_sp):
             g = lax.rem(sp + n_sp - d, n_sp)
             sel_arrival(c, g).wait_recv()
             relay_sel(c, g).start()
 
-        @pl.when(k > 0)
+        @pl.when(k < n_z - 1)
         def _():
             relay_x_in(c).wait_recv()
 
@@ -641,7 +724,7 @@
 
         @pl.when(k > 1)
         def _():
-            pass_on(lax.rem(z + k - 1, n_z))
+            pass_on(pick(out, z, k - 2))
 
         y_copy(c).wait_recv()
         sh_copy(c).wait_recv()
@@ -652,7 +735,7 @@
         return carry
 
     lax.fori_loop(0, n_z, step, 0)
-    pass_on(lax.rem(z + n_z - 1, n_z))
+    pass_on(pick(out, z, n_z - 2))
     fin[...] = combine(z)
     for d in range(1, n_z):
         c = lax.rem(z + d, n_z)
@@ -681,9 +764,10 @@
             q_copy(c, g).wait_send()
     for d in range(1, n_z):
         c = lax.rem(z + d, n_z)
-        z_copy(z, c).wait_send()
+        along(c, lambda copy: copy.wait_send())
         relay_x(c).wait_send()
         t_copy(c).wait_send()
+    along(z, lambda copy: copy.wait_send())
 
 
 def expert_shapes(n_sp, n_tp, rows, model, local, hidden, experts, capacity):
@@ -729,7 +813,7 @@
         in_specs=[inside] * 4 + [outside] * 6,
         out_specs=inside,
         scratch_shapes=[vm(shape, dtype) for shape, dtype in shapes]
-        + [dma((6,)), dma((2,)), one, one, one, one, two, two, two, two]
+        + [dma((6,)), dma((2,)), dma((2, n_z)), one, one, one, two, two, two, two]
         + [one, one, one, one, two, two, one, one, dma((2,))],
         compiler_params=pltpu.CompilerParams(
             collective_id=1, has_side_effects=True, vmem_limit_bytes=VMEM_LIMIT

time: 151 us -> 138 us (0.914)
  Pallas kernels: 149 us -> 136 us
    pallas_call x1, Pallas kernels: 93.9 us -> 84.9 us  [expert_layer(): pl.pallas_call(functools.partial(expert_kernel, (n_sp, n_tp, capacity)),...]
    pallas_call x1, Pallas kernels: 55 us -> 50.8 us  [mixer(): pl.pallas_call(functools.partial(mixer_kernel, (n_sp, n_tp, heads, capaci...]
where the time goes in v4:
time: 138 us; the launch traced here: 137 us
  Pallas kernels  136 us (99%)
  local copies, waits for them, and re-layouts  1.67 us (1%)
    pallas_call x1, Pallas kernels, expert_layer(): pl.pallas_call(functools.partial(expert_kernel, (n_sp, n_tp, capacity)),...  84.9 us
    pallas_call x1, Pallas kernels, mixer(): pl.pallas_call(functools.partial(mixer_kernel, (n_sp, n_tp, heads, capaci...  50.8 us

profile of v4, /device:TPU:0, one launch (start us, length us, event | category | flops | bytes accessed | tf_op | source)
XLA Modules:
  0.0 137.4 jit_solution(8544889362681316062)
XLA Ops:
  0.0 50.8 %shard_map.172 = (f32[64,2048]{1,0:T(8,128)}, f32[8,16,128]{2,1,0:T(8,128)}) custom-call(bf16[512,256]{1,0:T(8,128)(2,1)} %r_ref.1, bf16[512,256]{1,0:T(8,128)(2,1)} %k_ref.1, bf16[512,256]{1,0:T(8,128)(2,1)} %v_ref.1, bf16[512,256]{1,0:T(8,128)(2,1)} %e_ref.1, bf16[512,256]{1,0:T(8,128)(2,1)} %dp_ref.1, f32[4,512]{1,0:T(4,128)} %bitcast.3, ...), custom_call_target="tpu_custom_call" | custom-call | flops 10000000000 | bytes 10000000 | tf_op jit(solution)/shard_map/pallas_call | solution.py:470
  50.8 84.9 %shard_map.173 = bf16[64,2048]{1,0:T(8,128)(2,1)} custom-call(bf16[64,2048]{1,0:T(8,128)(2,1)} %input_ref.1, f32[64,2048]{1,0:T(8,128)} %get-tuple-element.7.projected_ref, bf16[2048]{0:T(1024)(128)(2,1)} %gain_ref.3, f32[8,16,128]{2,1,0:T(8,128)} %get-tuple-element.8.meta_ref, bf16[2,2048,512]{2,1,0:T(8,128)(2,1)} %gate_hbm.1, ...), custom_call_target="tpu_custom_call" | custom-call | flops 10000000000 | bytes 10000000 | tf_op jit(solution)/shard_map/pallas_call | solution.py:810
  135.7 1.7 %copy.20 = bf16[64,2048]{1,0:T(8,128)(2,1)} copy(bf16[64,2048]{1,0:T(8,128)(2,1)} %shard_map.173) | data formatting | bytes 524288

commit v5 on v4

--- a/solution.py
+++ b/solution.py
@@ -271,22 +271,6 @@
         send_maps[d] = whole[d].astype(BF16)
     pl.semaphore_wait(barrier, n_sp - 1 + n_tp - 1)
 
-    experts = meta_ref.shape[1] // 2
-    meta_s[tp] = route_table(routes_ref[...], rw_ref[...], experts, capacity, core)
-
-    def meta_copy(d):
-        return pltpu.make_async_remote_copy(
-            src_ref=meta_s.at[tp],
-            dst_ref=meta_s.at[tp],
-            send_sem=meta_send.at[d],
-            recv_sem=meta_recv.at[tp],
-            device_id=(sp, lax.rem(tp + d, n_tp)),
-            device_id_type=MESH,
-        )
-
-    for d in range(1, n_tp):
-        meta_copy(d).start()
-
     copies = []
     for d in range(1, n_sp):
         target = lax.rem(sp + d, n_sp)
@@ -300,6 +284,23 @@
         )
         copy.start()
         copies.append(copy)
+
+    experts = meta_ref.shape[1] // 2
+    meta_s[tp] = route_table(routes_ref[...], rw_ref[...], experts, capacity, core)
+
+    def meta_copy(d):
+        return pltpu.make_async_remote_copy(
+            src_ref=meta_s.at[tp],
+            dst_ref=meta_s.at[tp],
+            send_sem=meta_send.at[d],
+            recv_sem=meta_recv.at[tp],
+            device_id=(sp, lax.rem(tp + d, n_tp)),
+            device_id_type=MESH,
+        )
+
+    for d in range(1, n_tp):
+        meta_copy(d).start()
+
     for d in range(1, n_sp):
         source = lax.rem(sp + d, n_sp)
         pltpu.make_async_remote_copy(
@@ -405,18 +406,14 @@
         c = chip_at(i)
         there = pl.ds(pl.multiple_of(c * (2 * rows), 2 * rows), 2 * rows)
         first_block = c * (2 * rows // SPAN)
-        lax.fori_loop(first_block, first_block + 2 * rows // SPAN, finish, 0)
+        for n in range(2 * rows // SPAN):
+            finish(first_block + n, 0)
         part_s[c] = mul(mixed_s[there, :], w_ref[...]).astype(BF16)
         sib_copy(c).start()
-
-        @pl.when(i > 0)
-        def _():
-            pass_on(i - 1)
-
+        pass_on(i)
         return carry
 
     lax.fori_loop(0, n_z, project, 0)
-    pass_on(n_z - 1)
     for i in range(n_z - 1):
         c = chip_at(i)
 

time: 138 us -> 139 us (level)
  no operation moved by 1% of the time
where the time goes in v5:
time: 139 us
  Pallas kernels  137 us (99%)
  local copies, waits for them, and re-layouts  1.67 us (1%)
    pallas_call x1, Pallas kernels, expert_layer(): pl.pallas_call(functools.partial(expert_kernel, (n_sp, n_tp, capacity)),...  85.4 us
    pallas_call x1, Pallas kernels, mixer(): pl.pallas_call(functools.partial(mixer_kernel, (n_sp, n_tp, heads, capaci...  51.7 us

profile of v5, /device:TPU:0, one launch (start us, length us, event | category | flops | bytes accessed | tf_op | source)
XLA Modules:
  0.0 138.8 jit_solution(12700635552402959150)
XLA Ops:
  0.0 51.7 %shard_map.172 = (f32[64,2048]{1,0:T(8,128)}, f32[8,16,128]{2,1,0:T(8,128)}) custom-call(bf16[512,256]{1,0:T(8,128)(2,1)} %r_ref.1, bf16[512,256]{1,0:T(8,128)(2,1)} %k_ref.1, bf16[512,256]{1,0:T(8,128)(2,1)} %v_ref.1, bf16[512,256]{1,0:T(8,128)(2,1)} %e_ref.1, bf16[512,256]{1,0:T(8,128)(2,1)} %dp_ref.1, f32[4,512]{1,0:T(4,128)} %bitcast.3, ...), custom_call_target="tpu_custom_call" | custom-call | flops 10000000000 | bytes 10000000 | tf_op jit(solution)/shard_map/pallas_call | solution.py:467
  51.7 85.4 %shard_map.173 = bf16[64,2048]{1,0:T(8,128)(2,1)} custom-call(bf16[64,2048]{1,0:T(8,128)(2,1)} %input_ref.1, f32[64,2048]{1,0:T(8,128)} %get-tuple-element.7.projected_ref, bf16[2048]{0:T(1024)(128)(2,1)} %gain_ref.3, f32[8,16,128]{2,1,0:T(8,128)} %get-tuple-element.8.meta_ref, bf16[2,2048,512]{2,1,0:T(8,128)(2,1)} %gate_hbm.1, ...), custom_call_target="tpu_custom_call" | custom-call | flops 10000000000 | bytes 10000000 | tf_op jit(solution)/shard_map/pallas_call | solution.py:807
  137.1 1.7 %copy.20 = bf16[64,2048]{1,0:T(8,128)(2,1)} copy(bf16[64,2048]{1,0:T(8,128)(2,1)} %shard_map.173) | data formatting | bytes 524288
